TPU v7x, 512 devices: a whole 4x4x16 slice. The times are simulated.
512 devices in a mesh: sp: 64 (over z, y), tp: 8 (over x, core).
Axes of the slice: x: 4, y: 4, z: 16, core: 2. Of those that a mesh axis runs over, the one named last changes fastest.
Arguments:
- tokens: bfloat16 [16384, 2048], P('sp', 'tp'), may hold values from -6 to 6
- norm_gain: float32 [2048], replicated, may hold values from 0.1 to 1.9
- recv_weight: bfloat16 [2048, 1024], P(None, 'tp'), may hold values from -0.125 to 0.125
- lin_key_weight: bfloat16 [2048, 1024], P(None, 'tp'), may hold values from -0.125 to 0.125
- lin_value_weight: bfloat16 [2048, 1024], P(None, 'tp'), may hold values from -0.125 to 0.125
- decay_down: bfloat16 [2048, 64], replicated, may hold values from -0.125 to 0.125
- decay_up: bfloat16 [64, 1024], P(None, 'tp'), may hold values from -0.75 to 0.75
- decay_log_bias: float32 [1024], P('tp'), may hold values from -13 to -3
- decay_shift: float32 [16384, 1024], P('sp', 'tp'), may hold values from -1 to 13
- learn_rate: float32 [1024], P('tp'), may hold values from 0 to 1
- group_gain: float32 [1024], P('tp'), may hold values from 0.1 to 1.9
- initial_state: float32 [16, 64, 64], P('tp'), may hold values from -768 to 768
- query_weight: bfloat16 [2048, 1024], P(None, 'tp'), may hold values from -8 to 8
- att_key_weight: bfloat16 [2048, 1024], P(None, 'tp'), may hold values from -1 to 1
- att_value_weight: bfloat16 [2048, 1024], P(None, 'tp'), may hold values from -0.125 to 0.125
- gate_cache: float32 [16384, 8], P('sp', 'tp'), may hold values from -16384 to 0, as said below
- att_gain: float32 [1024], P('tp'), may hold values from 0.1 to 1.9
- out_lin_weight: bfloat16 [1024, 2048], P('tp'), may hold values from -0.125 to 0.125
- out_att_weight: bfloat16 [1024, 2048], P('tp'), may hold values from -0.125 to 0.125
Outputs:
- mixed_out: bfloat16 [16384, 2048], P('sp', 'tp')
Inputs may be any that keep to these rules, and one draw needn't show every extreme that they name: `gate_cache`: never rises along the sequence.
All inputs are finite; a program needn't handle non-finite values.
Results may differ from a plain program's by a relative error of at most 0.025.
Values may be sent and summed in bfloat16 or wider, within the bound.
No kernel may reach another device: no remote copies, remote signals or barrier semaphores. Data moves between devices by JAX's collectives and lax.ppermute only.
A program may use at most 64 MiB of HBM per device.

v0:
```python
import math

import jax
import jax.numpy as jnp
from jax import lax
from jax.sharding import Mesh
from jax.sharding import PartitionSpec as P

HEAD_LIN = 64
HEAD_ATT = 128
SP = ("sp_0", "sp_1")


def in_order(tiles, dim):
    tiles = jnp.moveaxis(tiles, 0, dim)
    dims = tiles.shape
    return tiles.reshape(*dims[:dim], dims[dim] * dims[dim + 1], *dims[dim + 2 :])


def from_everyone(shard, axis):
    size = lax.axis_size(axis)
    return lax.all_to_all(
        jnp.broadcast_to(shard[None], (size, *shard.shape)), axis, 0, 0, tiled=True
    )


def gather_directly(shard, axis, dim):
    return in_order(from_everyone(shard, axis), dim)


def filled_with(shard, identity):
    return jax.tree.map(
        lambda a, e: jnp.broadcast_to(jnp.asarray(e, a.dtype), a.shape), shard, identity
    )


def all_in_one(shard, axis):
    leaves = jax.tree.leaves(shard)
    turns = sorted(range(len(leaves)), key=lambda k: -leaves[k].size)
    width = (1, *leaves[turns[0]].shape)[-1]
    lines = [
        jnp.pad(leaves[k].reshape(-1), (0, -leaves[k].size % width)).reshape(-1, width)
        for k in turns
    ]
    both, at, found = (lax.all_gather(jnp.concatenate(lines), axis), 0, {})
    for k, line in zip(turns, lines):
        piece = both[:, at : at + len(line)].reshape(len(both), -1)
        found[k] = piece[:, : leaves[k].size].reshape(-1, *leaves[k].shape)
        at += len(line)
    numbers = iter(range(len(leaves)))
    return jax.tree.map(lambda _: found[next(numbers)], shard)


def carried_in(shard, axes, combine, identity):
    before = start = filled_with(shard, identity)
    subtotal = shard
    for axis in reversed(axes):
        size, place = (lax.axis_size(axis), lax.axis_index(axis))
        pieces = all_in_one(
            jax.tree.map(
                lambda part, kind: part.astype(kind), subtotal, (jnp.bfloat16, jnp.bfloat16)
            ),
            axis,
        )
        inside, subtotal = (start, start)
        for k in range(size):
            passed = k < place
            subtotal = combine(
                subtotal, jax.tree.map(lambda part, own: part[k].astype(own.dtype), pieces, shard)
            )
            inside = jax.tree.map(lambda new, old: jnp.where(passed, new, old), subtotal, inside)
        before = combine(inside, before)
    return before


def in_one_piece(arrays, axis, dim, along):
    ends, at = ([], 0)
    for a in arrays[:-1]:
        at += a.shape[along]
        ends.append(at)
    both = jnp.concatenate(arrays, axis=along)
    return tuple(jnp.split(lax.all_gather(both, axis, axis=dim, tiled=True), ends, axis=along))


def cut_along(shard, dim, size):
    dims = shard.shape
    tiles = shard.reshape(*dims[:dim], size, dims[dim] // size, *dims[dim + 1 :])
    return jnp.moveaxis(tiles, dim, 0)


def sent_and_summed(shard, axis, dim):
    size = lax.axis_size(axis)
    tiles = lax.all_to_all(cut_along(shard, dim, size), axis, 0, 0, tiled=True)
    return jnp.sum(tiles.astype(jnp.float32), axis=0)


def lin_advance(memory, inputs):
    decays, unit_key, rate_vec, key_now, value_now, recv_now = inputs
    along = jnp.einsum("hij,hj->hi", memory, unit_key)
    outer_add = value_now[:, :, None] * key_now[:, None, :]
    outer_add = jnp.concatenate([outer_add, jnp.zeros_like(outer_add)], axis=1)
    memory = memory * decays[:, None, :] - along[:, :, None] * rate_vec[:, None, :] + outer_add
    return (memory, jnp.einsum("hij,hj->hi", memory, recv_now))


def chain_combine(earlier, later):
    moved = jnp.einsum("hij,hjk->hik", earlier[0], later[0])
    shift_amounts = jnp.einsum("hij,hjk->hik", earlier[1], later[0]) + later[1]
    return (moved, shift_amounts)


def body(
    tokens,
    norm_gain,
    recv_weight,
    lin_key_weight,
    lin_value_weight,
    decay_down,
    decay_up,
    decay_log_bias,
    decay_shift,
    learn_rate,
    group_gain,
    initial_state,
    query_weight,
    att_key_weight,
    att_value_weight,
    gate_cache,
    att_gain,
    out_lin_weight,
    out_att_weight,
):
    tok_rows = tokens.shape[0]
    model_width = norm_gain.shape[0]
    weights = (
        recv_weight,
        lin_key_weight,
        lin_value_weight,
        query_weight,
        att_key_weight,
        att_value_weight,
        decay_down,
    )
    zeros_init = tuple((jnp.zeros((tok_rows, weight.shape[1]), jnp.float32) for weight in weights))
    pieces = gather_directly(tokens, "tp", 1)
    scaled = (pieces.astype(jnp.float32) * norm_gain).astype(jnp.bfloat16)
    partial_sums = tuple(
        (jnp.dot(scaled, weight, preferred_element_type=jnp.float32) for weight in weights)
    )
    projected = partial_sums + tuple((zeros_init + (jnp.zeros((tok_rows, 1), jnp.float32),))[7:])
    squares = jnp.sum(jnp.square(pieces.astype(jnp.float32)), axis=1, keepdims=True)
    projected = projected[:7] + (squares,)
    square_sum = projected[7]
    inverse = lax.rsqrt(square_sum / model_width + 1e-06)
    recv, lin_key, lin_value, queries, att_key, att_value, low_rank = (
        (total * inverse).astype(jnp.bfloat16) for total in projected[:7]
    )
    lin_heads = recv.shape[1] // HEAD_LIN
    exponent = (
        decay_log_bias
        + decay_shift
        + jnp.dot(
            jnp.tanh(low_rank.astype(jnp.float32)).astype(jnp.bfloat16),
            decay_up,
            preferred_element_type=jnp.float32,
        )
    )
    decays = jnp.exp(-jnp.exp(exponent))

    def heads_of(values):
        return values.astype(jnp.float32).reshape(tok_rows, lin_heads, HEAD_LIN)

    key_heads = heads_of(lin_key)
    unit_key = key_heads * lax.rsqrt(jnp.sum(key_heads * key_heads, axis=-1, keepdims=True) + 1e-06)
    rate_vec = unit_key * learn_rate.reshape(lin_heads, HEAD_LIN)
    identity = jnp.broadcast_to(
        jnp.eye(HEAD_LIN, dtype=jnp.float32), (lin_heads, HEAD_LIN, HEAD_LIN)
    )
    start_memory = jnp.concatenate([jnp.zeros_like(identity), identity], axis=1)
    inputs = (heads_of(decays), unit_key, rate_vec, key_heads, heads_of(lin_value), heads_of(recv))
    final_memory, outputs = lax.scan(lin_advance, start_memory, inputs, unroll=8)
    offset_now = final_memory[:, :HEAD_LIN]
    transfer_now = final_memory[:, HEAD_LIN:]
    prefix_map, prefix_add = carried_in(
        (transfer_now, offset_now), SP, chain_combine, (identity, jnp.zeros_like(identity))
    )
    incoming = jnp.einsum("hij,hjk->hik", initial_state, prefix_map) + prefix_add
    lin_raw = outputs[:, :, :HEAD_LIN] + jnp.einsum(
        "hij,thj->thi", incoming, outputs[:, :, HEAD_LIN:]
    )
    mean_val = jnp.mean(lin_raw, axis=-1, keepdims=True)
    spread_val = jnp.mean(jnp.square(lin_raw - mean_val), axis=-1, keepdims=True)
    lin_norm = (
        (lin_raw - mean_val)
        * lax.rsqrt(spread_val + 0.00064)
        * group_gain.reshape(lin_heads, HEAD_LIN)
    )
    lin_mixed = lin_norm.reshape(tok_rows, lin_heads * HEAD_LIN).astype(jnp.bfloat16)
    att_heads = queries.shape[1] // HEAD_ATT
    query_heads = queries.reshape(tok_rows, att_heads, HEAD_ATT)
    all_gates = gather_directly(gate_cache, SP, 0)
    query_pos = lax.axis_index(SP) * tok_rows + jnp.arange(tok_rows, dtype=jnp.int32)
    score_scale = HEAD_ATT ** (-0.5)
    query_gate = gate_cache.T
    start_state = (
        jnp.full((att_heads, tok_rows), -1e30, jnp.float32),
        jnp.zeros((att_heads, tok_rows), jnp.float32),
        jnp.zeros((att_heads, tok_rows, HEAD_ATT), jnp.float32),
    )
    key_heads_att = att_key.reshape(tok_rows, att_heads, HEAD_ATT)
    value_heads_att = att_value.reshape(tok_rows, att_heads, HEAD_ATT)
    running = start_state
    key_rows, value_rows = in_one_piece((key_heads_att, value_heads_att), SP, 0, 1)
    length = key_rows.shape[0]
    key_block = tok_rows * math.gcd(length // tok_rows, max(1, 1024 // tok_rows))
    blocks = length // key_block
    key_split = key_rows.reshape(blocks, key_block, att_heads, HEAD_ATT)
    value_split = value_rows.reshape(blocks, key_block, att_heads, HEAD_ATT)
    starts = jnp.arange(blocks, dtype=jnp.int32) * key_block

    def one_block(state_now, inputs_now):
        key_part, value_part, block_start = inputs_now

        def compute(held):
            best_score, totals, weighted = held
            key_gate = lax.dynamic_slice_in_dim(all_gates, block_start, key_block, 0)
            key_pos = block_start + jnp.arange(key_block, dtype=jnp.int32)
            allowed = key_pos[None, :] <= query_pos[:, None]
            logits = (
                jnp.einsum(
                    "qhd,khd->hqk", query_heads, key_part, preferred_element_type=jnp.float32
                )
                * score_scale
            )
            logits = logits + query_gate[:, :, None] - key_gate.T[:, None, :]
            logits = jnp.where(allowed[None], logits, -1e30)
            new_best = jnp.maximum(best_score, jnp.max(logits, axis=-1))
            raw_weights = jnp.where(allowed[None], jnp.exp(logits - new_best[..., None]), 0.0)
            factor = jnp.exp(best_score - new_best)
            totals = totals * factor + jnp.sum(raw_weights, axis=-1)
            weighted = weighted * factor[..., None] + jnp.einsum(
                "hqk,khd->hqd",
                raw_weights.astype(jnp.bfloat16),
                value_part,
                preferred_element_type=jnp.float32,
            )
            return (new_best, totals, weighted)

        def keep_running(held):
            return held

        return (lax.cond(block_start > query_pos[-1], keep_running, compute, state_now), None)

    running, _ = lax.scan(one_block, running, (key_split, value_split, starts))
    best_score, totals, weighted = running
    att_raw = weighted / totals[..., None]
    att_norm = (
        att_raw
        * lax.rsqrt(jnp.mean(att_raw * att_raw, axis=-1, keepdims=True) + 1e-06)
        * att_gain.reshape(att_heads, 1, HEAD_ATT)
    )
    att_mixed = (
        jnp.swapaxes(att_norm, 0, 1).reshape(tok_rows, att_heads * HEAD_ATT).astype(jnp.bfloat16)
    )
    partial_value = jnp.dot(lin_mixed, out_lin_weight, preferred_element_type=jnp.float32)
    partial_value = partial_value + jnp.dot(
        att_mixed, out_att_weight, preferred_element_type=jnp.float32
    )
    return sent_and_summed(partial_value.astype(jnp.bfloat16), "tp", 1).astype(jnp.bfloat16)


def solution(mesh):
    torus = Mesh(mesh.devices.reshape(16, 4, mesh.shape["tp"]), ("sp_0", "sp_1", "tp"))
    return jax.shard_map(
        body,
        mesh=torus,
        in_specs=(
            P(SP, "tp"),
            P(),
            P(None, "tp"),
            P(None, "tp"),
            P(None, "tp"),
            P(),
            P(None, "tp"),
            P("tp"),
            P(SP, "tp"),
            P("tp"),
            P("tp"),
            P("tp", None, None),
            P(None, "tp"),
            P(None, "tp"),
            P(None, "tp"),
            P(SP, "tp"),
            P("tp"),
            P("tp", None),
            P("tp", None),
        ),
        out_specs=P(SP, "tp"),
        check_vma=False,
    )
```

profile of v0, /device:TPU:480, one launch (start us, length us, event | category | flops | bytes accessed | tf_op | source)
XLA Modules:
  0.0 495.2 jit_solution(7788093297300624398)
XLA Ops:
  8.7 4.3 all-to-all-start
  14.5 14.4 %all-to-all-done = bf16[8,256,256]{1,2,0:T(8,128)(2,1)S(1)} async-done(((bf16[8,256,256]{1,2,0:T(8,128)(2,1)}), bf16[8,256,256]{1,2,0:T(8,128)(2,1)S(1)}, u32[]{:S(2)}, u32[]{:S(2)}) %all-to-all-start) | async-done | bytes 1048608 | tf_op jit(solution)/shard_map/all_to_all | solution.py:22
  30.2 12.3 %all-to-all-start.1 = ((f32[64,256,1]{1,2,0:T(1,128)}), f32[64,256,1]{1,2,0:T(1,128)S(1)}, u32[]{:S(2)}, u32[]{:S(2)}) async-start(f32[64,256,1]{1,2,0:T(1,128)} %broadcast_in_dim.105), calls=%async_computation.1 | async-start | bytes 131072 | tf_op jit(solution)/shard_map/all_to_all | solution.py:22
  43.3 1.4 fusion.77
  44.7 1.4 fusion.76
  46.9 1.4 fusion.69
  48.6 1.4 fusion.71
  54.5 209.6 %while.26 = (s32[]{:T(128)}, f32[2,128,64]{2,1,0:T(8,128)S(1)}, f32[32,8,2,128]{3,1,0,2:T(8,128)S(1)}, f32[32,8,2,64]{3,2,1,0:T(2,128)}, f32[32,8,2,64]{3,2,1,0:...) while((s32[]{:T(128)}, f32[2,128,64]{2,1,0:T(8,128)S(1)}, ...), condition=%wide.region_3.4_spmd, body=%wide.region_2.3_spmd.sunk | while | flops 1638409 | bytes 2507109 | solution.py:181
  264.8 12.6 %all-gather = bf16[1024,64]{1,0:T(8,128)(2,1)S(1)} all-gather(bf16[256,64]{1,0:T(8,128)(2,1)S(1)} %pad_maximum_fusion.1), channel_id=2, replica_groups=mesh['sp_0'=16,'sp_1'=4,'tp'=8] {'sp_1'}, dimensions={0}, use_global_device_ids=true | all-gather | bytes 163840 | tf_op jit(solution)/shard_map/all_gather | solution.py:45
  278.5 34.0 %all-gather.1 = bf16[4096,64]{1,0:T(8,128)(2,1)S(1)} all-gather(bf16[256,64]{1,0:T(8,128)(2,1)S(1)} %pad_maximum_fusion.2), channel_id=3, replica_groups=mesh['sp_0'=16,'sp_1'=4,'tp'=8] {'sp_0'}, dimensions={0}, use_global_device_ids=true | all-gather | bytes 557056 | tf_op jit(solution)/shard_map/all_gather | solution.py:45
  318.5 5.8 %fusion.169 = (bf16[16384,1,128]{0,2,1:T(8,128)(2,1)}, bf16[16384,1,128]{0,2,1:T(8,128)(2,1)}) fusion(bf16[16384,2,128]{0,2,1:T(8,128)(2,1)} %all-gather.4.cloned.1.call-done), kind=kLoop, calls=%fused_computation.290 | loop fusion | bytes 16777216 | tf_op jit(solution)/shard_map/split | solution.py:82
  324.3 6.4 %copy.133 = bf16[16384,1,128]{2,0,1:T(8,128)(2,1)} copy(bf16[16384,1,128]{0,2,1:T(8,128)(2,1)} %get-tuple-element.383) | data formatting | bytes 8388608 | tf_op jit(solution)/shard_map/while | solution.py:254
  330.7 6.4 %copy.132 = bf16[16384,1,128]{2,0,1:T(8,128)(2,1)} copy(bf16[16384,1,128]{0,2,1:T(8,128)(2,1)} %get-tuple-element.384) | data formatting | bytes 8388608 | tf_op jit(solution)/shard_map/while | solution.py:254
  337.2 131.2 %while.27 = (s32[]{:T(128)}, f32[1,256]{1,0:T(1,128)S(1)}, f32[1,256]{1,0:T(1,128)S(1)}, f32[1,256,128]{2,1,0:T(8,128)S(1)}, s32[16]{0:T(128)S(1)}, /*index=5*/s...) while((s32[]{:T(128)}, f32[1,256]{1,0:T(1,128)S(1)}, ...), condition=%wide.region_11.12_spmd, body=%wide.region_6.11_spmd.sunk | while | flops 137954816 | bytes 4048209 | solution.py:254
  339.6 5.8 %conditional.2 = (f32[1,256]{1,0:T(1,128)S(1)}, f32[1,256]{1,0:T(1,128)S(1)}, f32[1,256,128]{2,1,0:T(8,128)S(1)}) conditional(s32[]{:T(128)} %convert_element_type.374, (s32[]{:T(128)}, s32[256]{0:T(256)S(1)}, bf16[16,1024,1,128]{3,1,2,0:T(8,128)(2,1)}, s32[]{:T(128)}, bf16[256,1,128]{2,0,1:T(8,128)(2,1)S(1)}, /*index=5*/f32[256,1]{0,1:T(1,128)S(1)}, ...), branch_computations={%region_7.9_spmd, %region_10.10_spmd} | conditional | flops 137954816 | bytes 4045890 | solution.py:252
  342.2 1.4 fusion.168
  343.8 1.5 fusion.44
  347.8 5.8 %conditional.2 = (f32[1,256]{1,0:T(1,128)S(1)}, f32[1,256]{1,0:T(1,128)S(1)}, f32[1,256,128]{2,1,0:T(8,128)S(1)}) conditional(s32[]{:T(128)} %convert_element_type.374, (s32[]{:T(128)}, s32[256]{0:T(256)S(1)}, bf16[16,1024,1,128]{3,1,2,0:T(8,128)(2,1)}, s32[]{:T(128)}, bf16[256,1,128]{2,0,1:T(8,128)(2,1)S(1)}, /*index=5*/f32[256,1]{0,1:T(1,128)S(1)}, ...), branch_computations={%region_7.9_spmd, %region_10.10_spmd} | conditional | flops 137954816 | bytes 4045890 | solution.py:252
  352.0 1.5 fusion.44
  356.0 5.8 %conditional.2 = (f32[1,256]{1,0:T(1,128)S(1)}, f32[1,256]{1,0:T(1,128)S(1)}, f32[1,256,128]{2,1,0:T(8,128)S(1)}) conditional(s32[]{:T(128)} %convert_element_type.374, (s32[]{:T(128)}, s32[256]{0:T(256)S(1)}, bf16[16,1024,1,128]{3,1,2,0:T(8,128)(2,1)}, s32[]{:T(128)}, bf16[256,1,128]{2,0,1:T(8,128)(2,1)S(1)}, /*index=5*/f32[256,1]{0,1:T(1,128)S(1)}, ...), branch_computations={%region_7.9_spmd, %region_10.10_spmd} | conditional | flops 137954816 | bytes 4045890 | solution.py:252
  360.2 1.5 fusion.44
  364.2 5.8 %conditional.2 = (f32[1,256]{1,0:T(1,128)S(1)}, f32[1,256]{1,0:T(1,128)S(1)}, f32[1,256,128]{2,1,0:T(8,128)S(1)}) conditional(s32[]{:T(128)} %convert_element_type.374, (s32[]{:T(128)}, s32[256]{0:T(256)S(1)}, bf16[16,1024,1,128]{3,1,2,0:T(8,128)(2,1)}, s32[]{:T(128)}, bf16[256,1,128]{2,0,1:T(8,128)(2,1)S(1)}, /*index=5*/f32[256,1]{0,1:T(1,128)S(1)}, ...), branch_computations={%region_7.9_spmd, %region_10.10_spmd} | conditional | flops 137954816 | bytes 4045890 | solution.py:252
  368.4 1.5 fusion.44
  372.4 5.8 %conditional.2 = (f32[1,256]{1,0:T(1,128)S(1)}, f32[1,256]{1,0:T(1,128)S(1)}, f32[1,256,128]{2,1,0:T(8,128)S(1)}) conditional(s32[]{:T(128)} %convert_element_type.374, (s32[]{:T(128)}, s32[256]{0:T(256)S(1)}, bf16[16,1024,1,128]{3,1,2,0:T(8,128)(2,1)}, s32[]{:T(128)}, bf16[256,1,128]{2,0,1:T(8,128)(2,1)S(1)}, /*index=5*/f32[256,1]{0,1:T(1,128)S(1)}, ...), branch_computations={%region_7.9_spmd, %region_10.10_spmd} | conditional | flops 137954816 | bytes 4045890 | solution.py:252
  376.6 1.5 fusion.44
  380.6 5.8 %conditional.2 = (f32[1,256]{1,0:T(1,128)S(1)}, f32[1,256]{1,0:T(1,128)S(1)}, f32[1,256,128]{2,1,0:T(8,128)S(1)}) conditional(s32[]{:T(128)} %convert_element_type.374, (s32[]{:T(128)}, s32[256]{0:T(256)S(1)}, bf16[16,1024,1,128]{3,1,2,0:T(8,128)(2,1)}, s32[]{:T(128)}, bf16[256,1,128]{2,0,1:T(8,128)(2,1)S(1)}, /*index=5*/f32[256,1]{0,1:T(1,128)S(1)}, ...), branch_computations={%region_7.9_spmd, %region_10.10_spmd} | conditional | flops 137954816 | bytes 4045890 | solution.py:252
  384.8 1.5 fusion.44
  388.8 5.8 %conditional.2 = (f32[1,256]{1,0:T(1,128)S(1)}, f32[1,256]{1,0:T(1,128)S(1)}, f32[1,256,128]{2,1,0:T(8,128)S(1)}) conditional(s32[]{:T(128)} %convert_element_type.374, (s32[]{:T(128)}, s32[256]{0:T(256)S(1)}, bf16[16,1024,1,128]{3,1,2,0:T(8,128)(2,1)}, s32[]{:T(128)}, bf16[256,1,128]{2,0,1:T(8,128)(2,1)S(1)}, /*index=5*/f32[256,1]{0,1:T(1,128)S(1)}, ...), branch_computations={%region_7.9_spmd, %region_10.10_spmd} | conditional | flops 137954816 | bytes 4045890 | solution.py:252
  393.0 1.5 fusion.44
  397.0 5.8 %conditional.2 = (f32[1,256]{1,0:T(1,128)S(1)}, f32[1,256]{1,0:T(1,128)S(1)}, f32[1,256,128]{2,1,0:T(8,128)S(1)}) conditional(s32[]{:T(128)} %convert_element_type.374, (s32[]{:T(128)}, s32[256]{0:T(256)S(1)}, bf16[16,1024,1,128]{3,1,2,0:T(8,128)(2,1)}, s32[]{:T(128)}, bf16[256,1,128]{2,0,1:T(8,128)(2,1)S(1)}, /*index=5*/f32[256,1]{0,1:T(1,128)S(1)}, ...), branch_computations={%region_7.9_spmd, %region_10.10_spmd} | conditional | flops 137954816 | bytes 4045890 | solution.py:252
  401.2 1.5 fusion.44
  405.2 5.8 %conditional.2 = (f32[1,256]{1,0:T(1,128)S(1)}, f32[1,256]{1,0:T(1,128)S(1)}, f32[1,256,128]{2,1,0:T(8,128)S(1)}) conditional(s32[]{:T(128)} %convert_element_type.374, (s32[]{:T(128)}, s32[256]{0:T(256)S(1)}, bf16[16,1024,1,128]{3,1,2,0:T(8,128)(2,1)}, s32[]{:T(128)}, bf16[256,1,128]{2,0,1:T(8,128)(2,1)S(1)}, /*index=5*/f32[256,1]{0,1:T(1,128)S(1)}, ...), branch_computations={%region_7.9_spmd, %region_10.10_spmd} | conditional | flops 137954816 | bytes 4045890 | solution.py:252
  409.4 1.5 fusion.44
  413.4 5.8 %conditional.2 = (f32[1,256]{1,0:T(1,128)S(1)}, f32[1,256]{1,0:T(1,128)S(1)}, f32[1,256,128]{2,1,0:T(8,128)S(1)}) conditional(s32[]{:T(128)} %convert_element_type.374, (s32[]{:T(128)}, s32[256]{0:T(256)S(1)}, bf16[16,1024,1,128]{3,1,2,0:T(8,128)(2,1)}, s32[]{:T(128)}, bf16[256,1,128]{2,0,1:T(8,128)(2,1)S(1)}, /*index=5*/f32[256,1]{0,1:T(1,128)S(1)}, ...), branch_computations={%region_7.9_spmd, %region_10.10_spmd} | conditional | flops 137954816 | bytes 4045890 | solution.py:252
  417.6 1.5 fusion.44
  421.6 5.8 %conditional.2 = (f32[1,256]{1,0:T(1,128)S(1)}, f32[1,256]{1,0:T(1,128)S(1)}, f32[1,256,128]{2,1,0:T(8,128)S(1)}) conditional(s32[]{:T(128)} %convert_element_type.374, (s32[]{:T(128)}, s32[256]{0:T(256)S(1)}, bf16[16,1024,1,128]{3,1,2,0:T(8,128)(2,1)}, s32[]{:T(128)}, bf16[256,1,128]{2,0,1:T(8,128)(2,1)S(1)}, /*index=5*/f32[256,1]{0,1:T(1,128)S(1)}, ...), branch_computations={%region_7.9_spmd, %region_10.10_spmd} | conditional | flops 137954816 | bytes 4045890 | solution.py:252
  425.8 1.5 fusion.44
  429.8 5.8 %conditional.2 = (f32[1,256]{1,0:T(1,128)S(1)}, f32[1,256]{1,0:T(1,128)S(1)}, f32[1,256,128]{2,1,0:T(8,128)S(1)}) conditional(s32[]{:T(128)} %convert_element_type.374, (s32[]{:T(128)}, s32[256]{0:T(256)S(1)}, bf16[16,1024,1,128]{3,1,2,0:T(8,128)(2,1)}, s32[]{:T(128)}, bf16[256,1,128]{2,0,1:T(8,128)(2,1)S(1)}, /*index=5*/f32[256,1]{0,1:T(1,128)S(1)}, ...), branch_computations={%region_7.9_spmd, %region_10.10_spmd} | conditional | flops 137954816 | bytes 4045890 | solution.py:252
  434.0 1.5 fusion.44
  438.0 5.8 %conditional.2 = (f32[1,256]{1,0:T(1,128)S(1)}, f32[1,256]{1,0:T(1,128)S(1)}, f32[1,256,128]{2,1,0:T(8,128)S(1)}) conditional(s32[]{:T(128)} %convert_element_type.374, (s32[]{:T(128)}, s32[256]{0:T(256)S(1)}, bf16[16,1024,1,128]{3,1,2,0:T(8,128)(2,1)}, s32[]{:T(128)}, bf16[256,1,128]{2,0,1:T(8,128)(2,1)S(1)}, /*index=5*/f32[256,1]{0,1:T(1,128)S(1)}, ...), branch_computations={%region_7.9_spmd, %region_10.10_spmd} | conditional | flops 137954816 | bytes 4045890 | solution.py:252
  442.2 1.5 fusion.44
  446.2 5.8 %conditional.2 = (f32[1,256]{1,0:T(1,128)S(1)}, f32[1,256]{1,0:T(1,128)S(1)}, f32[1,256,128]{2,1,0:T(8,128)S(1)}) conditional(s32[]{:T(128)} %convert_element_type.374, (s32[]{:T(128)}, s32[256]{0:T(256)S(1)}, bf16[16,1024,1,128]{3,1,2,0:T(8,128)(2,1)}, s32[]{:T(128)}, bf16[256,1,128]{2,0,1:T(8,128)(2,1)S(1)}, /*index=5*/f32[256,1]{0,1:T(1,128)S(1)}, ...), branch_computations={%region_7.9_spmd, %region_10.10_spmd} | conditional | flops 137954816 | bytes 4045890 | solution.py:252
  450.4 1.5 fusion.44
  454.4 5.8 %conditional.2 = (f32[1,256]{1,0:T(1,128)S(1)}, f32[1,256]{1,0:T(1,128)S(1)}, f32[1,256,128]{2,1,0:T(8,128)S(1)}) conditional(s32[]{:T(128)} %convert_element_type.374, (s32[]{:T(128)}, s32[256]{0:T(256)S(1)}, bf16[16,1024,1,128]{3,1,2,0:T(8,128)(2,1)}, s32[]{:T(128)}, bf16[256,1,128]{2,0,1:T(8,128)(2,1)S(1)}, /*index=5*/f32[256,1]{0,1:T(1,128)S(1)}, ...), branch_computations={%region_7.9_spmd, %region_10.10_spmd} | conditional | flops 137954816 | bytes 4045890 | solution.py:252
  458.6 1.5 fusion.44
  462.6 5.8 %conditional.2 = (f32[1,256]{1,0:T(1,128)S(1)}, f32[1,256]{1,0:T(1,128)S(1)}, f32[1,256,128]{2,1,0:T(8,128)S(1)}) conditional(s32[]{:T(128)} %convert_element_type.374, (s32[]{:T(128)}, s32[256]{0:T(256)S(1)}, bf16[16,1024,1,128]{3,1,2,0:T(8,128)(2,1)}, s32[]{:T(128)}, bf16[256,1,128]{2,0,1:T(8,128)(2,1)S(1)}, /*index=5*/f32[256,1]{0,1:T(1,128)S(1)}, ...), branch_computations={%region_7.9_spmd, %region_10.10_spmd} | conditional | flops 137954816 | bytes 4045890 | solution.py:252
  466.8 1.5 fusion.44
  469.2 18.4 %all_to_all.15 = bf16[8,256,256]{2,1,0:T(8,128)(2,1)S(1)} all-to-all(bf16[8,256,256]{2,1,0:T(8,128)(2,1)S(1)} %bitcast.568), channel_id=1, replica_groups=mesh['sp_0'=16,'sp_1'=4,'tp'=8] {'tp'}, dimensions={0} | all-to-all | bytes 2097152 | tf_op jit(solution)/shard_map/all_to_all | solution.py:93
  (1544 shorter events, 281.9 us)
Async XLA Ops:
  6.5 311.5 %copy-start = (bf16[128,2048]{1,0:T(8,128)(2,1)S(1)}, bf16[128,2048]{1,0:T(8,128)(2,1)}, u32[]{:S(2)}) copy-start(bf16[128,2048]{1,0:T(8,128)(2,1)} %param.42) | copy-start | bytes 1572868
  6.5 36.4 %copy-start.8 = (f32[2048]{0:T(1024)S(1)}, f32[2048]{0:T(1024)}, u32[]{:S(2)}) copy-start(f32[2048]{0:T(1024)} %param.26) | copy-start | bytes 24580
  8.7 20.2 %all-to-all-start = ((bf16[8,256,256]{1,2,0:T(8,128)(2,1)}), bf16[8,256,256]{1,2,0:T(8,128)(2,1)S(1)}, u32[]{:S(2)}, u32[]{:S(2)}) async-start(bf16[8,256,256]{1,2,0:T(8,128)(2,1)} %broadcast_in_dim.100), calls=%async_computation | async-start | bytes 2097152 | tf_op jit(solution)/shard_map/all_to_all | solution.py:22
  30.2 306.9 %all-to-all-start.1 = ((f32[64,256,1]{1,2,0:T(1,128)}), f32[64,256,1]{1,2,0:T(1,128)S(1)}, u32[]{:S(2)}, u32[]{:S(2)}) async-start(f32[64,256,1]{1,2,0:T(1,128)} %broadcast_in_dim.105), calls=%async_computation.1 | async-start | bytes 131072 | tf_op jit(solution)/shard_map/all_to_all | solution.py:22
  42.5 276.0 %all-gather.4.cloned.1.call-start = ((), (), s32[]{:S(2)}) async-start(), calls=%async_computation.3 | async-start | bytes 8519680 | tf_op jit(solution)/shard_map/all_gather | solution.py:82
  43.3 7.7 %copy-start.2 = (bf16[2048,128]{1,0:T(8,128)(2,1)S(1)}, bf16[2048,128]{1,0:T(8,128)(2,1)}, u32[]{:S(2)}) copy-start(bf16[2048,128]{1,0:T(8,128)(2,1)} %param.28) | copy-start | bytes 1572868
  46.1 5.7 %copy-start.4 = (bf16[2048,64]{0,1:T(8,128)(2,1)S(1)}, bf16[2048,64]{0,1:T(8,128)(2,1)}, u32[]{:S(2)}) copy-start(bf16[2048,64]{0,1:T(8,128)(2,1)} %param.30) | copy-start | bytes 786436
  46.1 5.7 %copy-start.5 = (f32[256,128]{1,0:T(8,128)S(1)}, f32[256,128]{1,0:T(8,128)}, u32[]{:S(2)}) copy-start(f32[256,128]{1,0:T(8,128)} %param.33) | copy-start | bytes 393220
  46.1 5.7 %copy-start.7 = (bf16[64,128]{1,0:T(8,128)(2,1)S(1)}, bf16[64,128]{1,0:T(8,128)(2,1)}, u32[]{:S(2)}) copy-start(bf16[64,128]{1,0:T(8,128)(2,1)} %param.31) | copy-start | bytes 49156
  46.2 5.7 %copy-start.10 = (f32[128]{0:T(128)S(1)}, f32[128]{0:T(128)}, u32[]{:S(2)}) copy-start(f32[128]{0:T(128)} %param.32) | copy-start | bytes 1540
  54.5 209.6 %copy-start.3 = (bf16[2048,128]{1,0:T(8,128)(2,1)S(1)}, bf16[2048,128]{1,0:T(8,128)(2,1)}, u32[]{:S(2)}) copy-start(bf16[2048,128]{1,0:T(8,128)(2,1)} %param.37) | copy-start | bytes 1572868
  278.0 38.9 %copy-start.6 = (f32[2,64,64]{2,1,0:T(8,128)S(1)}, f32[2,64,64]{2,1,0:T(8,128)}, u32[]{:S(2)}) copy-start(f32[2,64,64]{2,1,0:T(8,128)} %param.36) | copy-start | bytes 98308
  330.7 6.5 %copy-start.9 = (f32[256,1]{0,1:T(1,128)S(1)}, f32[256,1]{0,1:T(1,128)}, u32[]{:S(2)}) copy-start(f32[256,1]{0,1:T(1,128)} %param.40) | copy-start | bytes 3076
  337.2 131.4 %copy-start.1 = (bf16[128,2048]{1,0:T(8,128)(2,1)S(1)}, bf16[128,2048]{1,0:T(8,128)(2,1)}, u32[]{:S(2)}) copy-start(bf16[128,2048]{1,0:T(8,128)(2,1)} %param.43) | copy-start | bytes 1572868
  337.2 131.4 %copy-start.11 = (f32[128]{0:T(128)S(1)}, f32[128]{0:T(128)}, u32[]{:S(2)}) copy-start(f32[128]{0:T(128)} %param.41) | copy-start | bytes 1540
Sparse Core Ops, SparseCore 0:
  47.0 166.2 all-gather.3
where the time goes:
time: 499 us; the launch traced here: 495 us
  matrix products  153 us (31%)
  local copies, waits for them, and re-layouts  122 us (24%)
  blocking collectives  65 us (13%)
  other arithmetic  56.7 us (11%)
  loops' own time  53.2 us (11%)
  starting transfers between devices  16.6 us (3%)
  waiting for transfers between devices  14.4 us (3%)
  between operations  13.9 us (3%)
    all_gather x2, blocking collectives, all_in_one(): both, at, found = (lax.all_gather(jnp.concatenate(lines), axis), 0, {})  46.6 us
    dot_general x256, matrix products, lin_advance(): return (memory, jnp.einsum('hij,hj->hi', memory, recv_now))  46.6 us
    dot_general x256, matrix products, lin_advance(): along = jnp.einsum('hij,hj->hi', memory, unit_key)  46.4 us
    another operation x16, loops' own time, one_block(): lax.cond(block_start > query_pos[-1], keep_running, compute, state_now)  30.3 us
    dot_general x16, matrix products, compute(): jnp.einsum('hqk,khd->hqd', raw_weights.astype(jnp.bfloat16), value_part,...  24.6 us
    slice x32, local copies, waits for them, and re-layouts, body(): lax.scan(lin_advance, start_memory, inputs, unroll=8)  24.6 us
    mul x32, local copies, waits for them, and re-layouts, lin_advance(): outer_add = value_now[:, :, None] * key_now[:, None, :]  23.6 us
    mul x32, local copies, waits for them, and re-layouts, lin_advance(): memory * decays[:, None, :] - along[:, :, None] * rate_vec[:, None, :]  23.5 us
  transfers between devices with their start and end apart: 3, of which 1 were waited for; matrix products, arithmetic and copies ran while one was open for 50% of the time, Pallas kernels for 0%

commit v1 on v0

v1 whole, which is shorter than its diff:
```python
import functools
import math

import jax
import jax.numpy as jnp
from jax import lax
from jax.experimental import pallas as pl
from jax.experimental.pallas import tpu as pltpu
from jax.sharding import Mesh
from jax.sharding import PartitionSpec as P

HEAD_LIN = 64
HEAD_ATT = 128
WIDE = 128
SP = ("z", "y")
TP = ("x", "c")
LOG2E = math.log2(math.e)
NEG = -1e30
F32 = jnp.float32
BF16 = jnp.bfloat16


def params():
    return pltpu.CompilerParams(vmem_limit_bytes=48 * 1024 * 1024)


def cost(flops, size):
    return pl.CostEstimate(flops=flops, bytes_accessed=size, transcendentals=0)


def dot(a, b, dims=((1,), (0,))):
    return lax.dot_general(a, b, (dims, ((), ())), preferred_element_type=F32)


def parts_of(a):
    high = a.astype(BF16)
    return high, (a - high.astype(F32)).astype(BF16)


def dot3(a, b, dims=((1,), (0,))):
    ah, al = parts_of(a)
    bh, bl = parts_of(b)
    return dot(ah, bh, dims) + (dot(ah, bl, dims) + dot(al, bh, dims))


def dot2(a, b, dims=((1,), (0,))):
    ah, al = parts_of(a)
    return dot(ah, b, dims) + dot(al, b, dims)


def iota(shape, dim):
    return lax.broadcasted_iota(jnp.int32, shape, dim)


def by_head(a):
    left = iota(a.shape, 1) < HEAD_LIN
    first = jnp.sum(jnp.where(left, a, 0.0), axis=1, keepdims=True)
    second = jnp.sum(jnp.where(left, 0.0, a), axis=1, keepdims=True)
    return jnp.where(left, first, second)


def scaled_pieces(pieces_ref, gain_ref):
    shards, rows, depth = pieces_ref.shape
    scaled, squares = [], jnp.zeros((rows, depth), F32)
    for j in range(shards):
        wide = pieces_ref[j].astype(F32)
        scaled.append((wide * gain_ref[:, j * depth : (j + 1) * depth]).astype(BF16))
        squares = squares + wide * wide
    mean = jnp.sum(squares, axis=1, keepdims=True) / (shards * depth)
    return scaled, lax.rsqrt(mean + 1e-6)


def projected(scaled, inverse, w_ref):
    depth = scaled[0].shape[1]
    total = dot(scaled[0], w_ref[0:depth])
    for j in range(1, len(scaled)):
        total = total + dot(scaled[j], w_ref[j * depth : (j + 1) * depth])
    return (total * inverse).astype(BF16)


def kv_kernel(pieces_ref, gain_ref, wk_ref, wv_ref, out_ref):
    scaled, inverse = scaled_pieces(pieces_ref, gain_ref)
    out_ref[:, :HEAD_ATT] = projected(scaled, inverse, wk_ref)
    out_ref[:, HEAD_ATT:] = projected(scaled, inverse, wv_ref)


def spans(log_decay):
    rows = log_decay.shape[0]
    row = iota(log_decay.shape, 0)
    zero = jnp.zeros_like(log_decay)
    before = [None] + [pltpu.roll(log_decay, i, 0) for i in range(1, 8)]
    behind = [None] + [pltpu.roll(log_decay, rows - i, 0) for i in range(1, 8)]
    ahead, after = {1: zero}, {1: zero}
    for h in (2, 4, 8):
        place = row & (h - 1)
        a, b = zero, zero
        for i in range(1, h):
            a = a + jnp.where(place >= i, before[i], 0.0)
            b = b + jnp.where(place + i < h, behind[i], 0.0)
        ahead[h], after[h] = a, b
    h = 8
    while h < rows:
        shape = (rows // (2 * h), 2 * h, WIDE)
        a, b = ahead[h].reshape(shape), after[h].reshape(shape)
        step = log_decay.reshape(shape)
        left = a[:, h - 1 : h] + step[:, h - 1 : h]
        right = b[:, h : h + 1] + step[:, h : h + 1]
        a = jnp.concatenate([a[:, :h], a[:, h:] + left], axis=1)
        b = jnp.concatenate([b[:, :h] + right, b[:, h:]], axis=1)
        h *= 2
        ahead[h], after[h] = a.reshape(rows, WIDE), b.reshape(rows, WIDE)
    return ahead, after


def lin_kernel(
    pieces_ref,
    gain_ref,
    wr_ref,
    wk_ref,
    wv_ref,
    wq_ref,
    down_ref,
    up_ref,
    bias_ref,
    shift_ref,
    rate_ref,
    gate_ref,
    send_ref,
    gates_ref,
    reach_ref,
    local_ref,
    pairs_ref,
):
    scaled, inverse = scaled_pieces(pieces_ref, gain_ref)
    rows = shift_ref.shape[0]
    send_ref[0:rows] = projected(scaled, inverse, wq_ref)
    recv = projected(scaled, inverse, wr_ref).astype(F32)
    key = projected(scaled, inverse, wk_ref).astype(F32)
    value = projected(scaled, inverse, wv_ref)
    low = projected(scaled, inverse, down_ref).astype(F32)
    exponent = bias_ref[...] + shift_ref[...] + dot(jnp.tanh(low).astype(BF16), up_ref[...])
    log_decay = -jnp.exp(exponent)
    unit = key * lax.rsqrt(by_head(key * key) + 1e-6)
    rate = unit * rate_ref[...]

    ahead, after = spans(log_decay)
    lane = iota((rows, WIDE), 1)
    row = iota((rows, WIDE), 0)
    tall = iota((rows, rows), 0)
    flat = iota((rows, rows), 1)
    heads = [lane < HEAD_LIN, lane >= HEAD_LIN]

    def of_heads(a):
        return [jnp.where(mine, a, 0.0).astype(BF16) for mine in heads]

    eye = tall == flat
    right_now = jnp.concatenate([key, rate], axis=0).astype(BF16)
    for n, q_part in enumerate(of_heads(recv)):
        product = dot(q_part, right_now, ((1,), (1,)))
        for m in range(2):
            mine = slice(m * rows, (m + 1) * rows)
            pairs_ref[n, 1, :, mine] = jnp.where(eye, product[:, mine], 0.0)
            pairs_ref[n, 0, :, mine] = jnp.zeros((rows, rows), F32)
    h, level = 1, 0
    while h < rows:
        late = (row & h) != 0
        to_u = jnp.where(late, jnp.exp(ahead[h]), 0.0)
        to_q = jnp.where(late, jnp.exp(ahead[h] + log_decay), 0.0)
        from_s = jnp.where(late, 0.0, jnp.exp(after[h]))
        right = jnp.concatenate([key * from_s, rate * from_s], axis=0).astype(BF16)
        left = of_heads(unit * to_u), of_heads(recv * to_q)
        here = ((tall >> (level + 1)) == (flat >> (level + 1))) & ((tall & h) != 0) & (
            (flat & h) == 0
        )
        for n in range(2):
            for k in range(2):
                product = dot(left[k][n], right, ((1,), (1,)))
                for m in range(2):
                    mine = slice(m * rows, (m + 1) * rows)
                    pairs_ref[n, k, :, mine] = jnp.where(
                        here, product[:, mine], pairs_ref[n, k, :, mine]
                    )
        h *= 2
        level += 1

    solved = [jnp.where(eye, 1.0, 0.0) for _ in range(2)]
    h, level = 1, 0
    while h < rows:
        here = ((tall >> (level + 1)) == (flat >> (level + 1))) & ((tall & h) != 0) & (
            (flat & h) == 0
        )
        for n in range(2):
            links = jnp.where(here, pairs_ref[n, 0, :, rows:], 0.0)
            if h == 1:
                solved[n] = solved[n] - links
            else:
                step = dot3(links, solved[n])
                solved[n] = solved[n] - dot3(solved[n], step)
        h *= 2
        level += 1

    full_u = unit * jnp.exp(ahead[rows])
    full_q = recv * jnp.exp(ahead[rows] + log_decay)
    tail = jnp.exp(after[rows])
    full_k = key * tail
    full_r = rate * tail
    reach, local, moved = [], [], []
    for n in range(2):
        add = dot2(pairs_ref[n, 0, :, :rows], value)
        source = jnp.where(heads[n], full_u, pltpu.roll(add, HEAD_LIN, 1))
        along = dot3(solved[n], source)
        taken = dot3(pairs_ref[n, 1, :, rows:], along)
        reach.append(full_q - taken)
        local.append(dot2(pairs_ref[n, 1, :, :rows], value) - pltpu.roll(taken, HEAD_LIN, 1))
        moved.append(dot3(along, full_r, ((0,), (0,))))
    reach_ref[...] = jnp.where(heads[0], reach[0], reach[1])
    local_ref[...] = jnp.where(heads[0], local[0], local[1])

    lane = iota((WIDE, WIDE), 1)
    row = iota((WIDE, WIDE), 0)
    same = (lane < HEAD_LIN) == (row < HEAD_LIN)
    added = pltpu.roll(dot2(full_k, value, ((0,), (0,))).T, HEAD_LIN, 0)
    last = jnp.exp(ahead[rows][rows - 1 : rows] + log_decay[rows - 1 : rows]) - 1.0
    packed = jnp.where(same, jnp.where(lane == row, last, 0.0), added)
    packed = packed - jnp.where(lane < HEAD_LIN, moved[0], moved[1])
    send_ref[rows : rows + WIDE] = packed.astype(BF16)
    gate = gate_ref[...]
    high, mid = parts_of(gate)
    low_part = (gate - high.astype(F32) - mid.astype(F32)).astype(BF16)
    none = jnp.zeros((10, WIDE), BF16)
    gates = jnp.concatenate([high, mid, low_part, none], axis=0)
    send_ref[rows + WIDE :] = gates
    gates_ref[...] = gates


def unpacked(packed):
    packed = packed.astype(F32)
    lane = iota((WIDE, WIDE), 1)
    row = iota((WIDE, WIDE), 0)
    same = (lane < HEAD_LIN) == (row < HEAD_LIN)
    return jnp.where(same, packed, 0.0), jnp.where(same, pltpu.roll(packed, HEAD_LIN, 0), 0.0)


def row_kernel(place_ref, gathered_ref, gates_ref, send_ref, before_ref, *, rows):
    y = place_ref[1]
    count = gathered_ref.shape[0]
    shape = (WIDE, WIDE)
    total = jnp.zeros(shape, F32), jnp.zeros(shape, F32)
    mine = total
    for j in range(count):
        mine = tuple(jnp.where(y == j, t, m) for t, m in zip(total, mine))
        moved, added = unpacked(gathered_ref[j, rows : rows + WIDE])
        if j == 0:
            total = moved, added
        else:
            total = (
                total[0] + moved + dot3(total[0], moved),
                total[1] + added + dot3(total[1], moved),
            )
    before_ref[0] = mine[0]
    before_ref[1] = mine[1]
    lane = iota(shape, 1)
    row = iota(shape, 0)
    same = (lane < HEAD_LIN) == (row < HEAD_LIN)
    packed = jnp.where(same, total[0], pltpu.roll(total[1], HEAD_LIN, 0))
    send_ref[0:WIDE] = packed.astype(BF16)
    send_ref[WIDE:] = gates_ref[...]


def mix_kernel(place_ref, state_ref, gathered_ref, before_ref, reach_ref, local_ref, gain_ref, out_ref):
    z = place_ref[0]
    none = jnp.zeros((HEAD_LIN, HEAD_LIN), F32)
    state = jnp.concatenate(
        [
            jnp.concatenate([state_ref[0], none], axis=1),
            jnp.concatenate([none, state_ref[1]], axis=1),
        ],
        axis=0,
    )

    def step(k, state):
        packed = gathered_ref[k]
        moved, added = unpacked(packed[0:WIDE])
        return state + dot2(state, moved.astype(BF16)) + added

    state = lax.fori_loop(0, z, step, state)
    state = state + dot3(state, before_ref[0]) + before_ref[1]
    raw = dot3(reach_ref[...], state, ((1,), (1,))) + local_ref[...]
    off = raw - by_head(raw) * (1.0 / HEAD_LIN)
    spread = by_head(off * off) * (1.0 / HEAD_LIN)
    out_ref[...] = (off * lax.rsqrt(spread + 0.00064) * gain_ref[...]).astype(BF16)


def joined(gates):
    gates = gates.astype(F32)
    return gates[0:2] + gates[2:4] + gates[4:6]


def att_kernel(place_ref, asked_ref, held_ref, keys_ref, out_ref, best_ref, sum_ref, *, rows):
    z, y = place_ref[0], place_ref[1]
    count = asked_ref.shape[0]
    scale = HEAD_ATT ** (-0.5) * LOG2E
    best_ref[...] = jnp.full(best_ref.shape, NEG, F32)
    sum_ref[...] = jnp.zeros(sum_ref.shape, F32)
    ones = jnp.ones((rows, HEAD_ATT), BF16)
    zero_gate = [joined(asked_ref[j, rows + WIDE : rows + WIDE + 16])[0:1, 0:1] for j in range(count)]

    def block(k, masked):
        start = pl.multiple_of(k * rows, rows)
        both = keys_ref[pl.ds(start, rows)]
        key = both[:, :HEAD_ATT]
        value = jnp.concatenate([both[:, HEAD_ATT:], ones], axis=1)
        gate = joined(held_ref[k][WIDE : WIDE + 16])
        gate = jnp.concatenate([gate[0:1], gate[1:2]], axis=1)
        for j in range(count):
            logits = dot(asked_ref[j, 0:rows], key, ((1,), (1,))) * scale
            logits = logits + (zero_gate[j] - gate) * LOG2E
            if masked:
                allowed = y * rows + iota(logits.shape, 1) <= j * rows + iota(logits.shape, 0)
                logits = jnp.where(allowed, logits, NEG)
            old = best_ref[j][:, 0:1]
            new = jnp.maximum(old, jnp.max(logits, axis=1, keepdims=True))
            weights = jnp.exp2(logits - new)
            if masked:
                weights = jnp.where(allowed, weights, 0.0)
            sum_ref[j] = sum_ref[j] * jnp.exp2(old - new) + dot(weights.astype(BF16), value)
            best_ref[j] = jnp.broadcast_to(new, (rows, WIDE))

    lax.fori_loop(0, z, lambda k, c: (block(k, False), c)[1], 0)
    block(z, True)
    third = iota((rows, WIDE), 1)
    for j in range(count):
        total = sum_ref[j][:, HEAD_ATT:]
        some = total > 0.0
        safe = jnp.where(some, total, 1.0)
        out_ref[j, :, :HEAD_ATT] = (sum_ref[j][:, :HEAD_ATT] / safe).astype(BF16)
        level = jnp.where(some, best_ref[j] + jnp.log(safe) * LOG2E, NEG)
        high, mid = parts_of(level)
        last = (level - high.astype(F32) - mid.astype(F32)).astype(BF16)
        level = jnp.where(third < 40, high.astype(F32), jnp.where(third < 80, mid.astype(F32), last.astype(F32)))
        out_ref[j, :, HEAD_ATT:] = level.astype(BF16)


def out_kernel(parts_ref, lin_ref, gain_ref, wl_ref, wa_ref, out_ref):
    count, rows = parts_ref.shape[0], parts_ref.shape[1]
    levels = []
    for j in range(count):
        level = parts_ref[j, :, HEAD_ATT:].astype(F32)
        levels.append(level[:, 0:1] + level[:, 40:41] + level[:, 80:81])
    top = functools.reduce(jnp.maximum, levels)
    total, raw = jnp.zeros((rows, 1), F32), jnp.zeros((rows, HEAD_ATT), F32)
    for j in range(count):
        share = jnp.exp2(levels[j] - top)
        total = total + share
        raw = raw + share * parts_ref[j, :, :HEAD_ATT].astype(F32)
    raw = raw / total
    size = jnp.mean(raw * raw, axis=1, keepdims=True)
    att = (raw * lax.rsqrt(size + 1e-6) * gain_ref[...]).astype(BF16)
    lin = lin_ref[...]
    width = out_ref.shape[2]
    for j in range(out_ref.shape[0]):
        mine = slice(j * width, (j + 1) * width)
        out_ref[j] = (dot(lin, wl_ref[:, mine]) + dot(att, wa_ref[:, mine])).astype(BF16)


def sent_to_all(a, axis):
    size = lax.axis_size(axis)
    return lax.all_to_all(jnp.broadcast_to(a[None], (size, *a.shape)), axis, 0, 0, tiled=True)


def smem():
    return pl.BlockSpec(memory_space=pltpu.SMEM)


def vmem():
    return pl.BlockSpec(memory_space=pltpu.VMEM)


def call(kernel, name, shapes, flops, size, scratch=(), scalars=0):
    def run(*operands):
        many = isinstance(shapes, (list, tuple))
        return pl.pallas_call(
            kernel,
            name=name,
            out_shape=shapes,
            in_specs=[smem()] * scalars + [vmem()] * (len(operands) - scalars),
            out_specs=[vmem()] * len(shapes) if many else vmem(),
            scratch_shapes=list(scratch),
            compiler_params=params(),
            cost_estimate=cost(flops, size),
        )(*operands)

    return run


def body(
    tokens,
    norm_gain,
    recv_weight,
    lin_key_weight,
    lin_value_weight,
    decay_down,
    decay_up,
    decay_log_bias,
    decay_shift,
    learn_rate,
    group_gain,
    initial_state,
    query_weight,
    att_key_weight,
    att_value_weight,
    gate_cache,
    att_gain,
    out_lin_weight,
    out_att_weight,
):
    rows = tokens.shape[0]
    nz, ny = lax.axis_size("z"), lax.axis_size("y")
    ntp = lax.axis_size(TP)
    model_width = norm_gain.shape[0]
    shape = jax.ShapeDtypeStruct
    place = jnp.stack([lax.axis_index("z"), lax.axis_index("y")]).astype(jnp.int32)
    gain = norm_gain.reshape(1, -1)

    pieces = sent_to_all(tokens, TP)
    kv = call(kv_kernel, "kv", shape((rows, 256), BF16), 2 * rows * model_width * 256, 1 << 21)(
        pieces, gain, att_key_weight, att_value_weight
    )
    keys = lax.all_gather(kv, "z", axis=0, tiled=True)

    extra = 16
    send, gates, reach, local = call(
        lin_kernel,
        "lin",
        (
            shape((rows + WIDE + extra, WIDE), BF16),
            shape((extra, WIDE), BF16),
            shape((rows, WIDE), F32),
            shape((rows, WIDE), F32),
        ),
        4 * 10**9,
        1 << 22,
        scratch=[pltpu.VMEM((2, 2, rows, 2 * rows), F32)],
    )(
        pieces,
        gain,
        recv_weight,
        lin_key_weight,
        lin_value_weight,
        query_weight,
        decay_down,
        decay_up,
        decay_log_bias.reshape(1, -1),
        decay_shift,
        learn_rate.reshape(1, -1),
        gate_cache.reshape(rows // WIDE, WIDE),
    )
    asked = sent_to_all(send, "y")
    row_send, before = call(
        functools.partial(row_kernel, rows=rows),
        "row",
        (shape((WIDE + extra, WIDE), BF16), shape((2, WIDE, WIDE), F32)),
        10**8,
        1 << 20,
        scalars=1,
    )(place, asked, gates)
    held = sent_to_all(row_send, "z")
    lin_mixed = call(
        mix_kernel, "mix", shape((rows, WIDE), BF16), 10**9, 1 << 20, scalars=1
    )(place, initial_state, held, before, reach, local, group_gain.reshape(1, -1))
    found = call(
        functools.partial(att_kernel, rows=rows),
        "att",
        shape((ny, rows, 256), BF16),
        ny * rows * nz * rows * 512,
        1 << 22,
        scratch=[
            pltpu.VMEM((ny, rows, WIDE), F32),
            pltpu.VMEM((ny, rows, 256), F32),
        ],
        scalars=1,
    )(place, asked, held, keys)
    parts = lax.all_to_all(found, "y", 0, 0, tiled=True)
    width = model_width // ntp
    partial = call(
        out_kernel, "out", shape((ntp, rows, width), BF16), 2 * rows * 256 * model_width, 1 << 21
    )(parts, lin_mixed, att_gain.reshape(1, -1), out_lin_weight, out_att_weight)
    tiles = lax.all_to_all(partial, TP, 0, 0, tiled=True)
    return jnp.sum(tiles.astype(F32), axis=0).astype(BF16)


def solution(mesh):
    sp, tp = mesh.shape["sp"], mesh.shape["tp"]
    cores = 2
    ny = math.isqrt(sp) // 2 if sp > 16 else 2
    torus = Mesh(mesh.devices.reshape(sp // ny, ny, tp // cores, cores), SP + TP)
    return jax.shard_map(
        body,
        mesh=torus,
        in_specs=(
            P(SP, TP),
            P(),
            P(None, TP),
            P(None, TP),
            P(None, TP),
            P(),
            P(None, TP),
            P(TP),
            P(SP, TP),
            P(TP),
            P(TP),
            P(TP, None, None),
            P(None, TP),
            P(None, TP),
            P(None, TP),
            P(SP, TP),
            P(TP),
            P(TP, None),
            P(TP, None),
        ),
        out_specs=P(SP, TP),
        check_vma=False,
    )
```

time: 499 us -> 187 us (0.37)
  matrix products: 153 us -> 0 us
  local copies, waits for them, and re-layouts: 122 us -> 7.54 us
  other arithmetic: 56.7 us -> 0.89 us
  loops' own time: 53.2 us -> 0 us
  Pallas kernels: 0 us -> 47.2 us
  blocking collectives: 65 us -> 88 us
  starting transfers between devices: 16.6 us -> 8.77 us
  waiting for transfers between devices: 14.4 us -> 20 us
    dot_general x596 -> x0, matrix products: 153 us -> none  [the longest x256 46.6 us: lin_advance(): return (memory, jnp.einsum('hij,hj->hi', memory, recv_now))]
    all_to_all x1 -> x3, blocking collectives: 18.4 us -> 88 us  [the longest x2 67.8 us: sent_to_all(): lax.all_to_all(jnp.broadcast_to(a[None], (size, *a.shape)), axis, 0, 0, t...]
    another operation x18 -> x0, loops' own time: 53.2 us -> none  [the longest x16 30.3 us: one_block(): lax.cond(block_start > query_pos[-1], keep_running, compute, state_now)]
    mul x66 -> x0, local copies, waits for them, and re-layouts: 48.6 us -> none  [the longest x32 23.6 us: lin_advance(): outer_add = value_now[:, :, None] * key_now[:, None, :]]
    pallas_call x0 -> x6, Pallas kernels: none -> 47.2 us  [run(): pl.pallas_call(kernel, name=name, out_shape=shapes, in_specs=[smem()] * s...]
    all_gather x2 -> x0, blocking collectives: 46.6 us -> none  [all_in_one(): both, at, found = (lax.all_gather(jnp.concatenate(lines), axis), 0, {})]
    slice x52 -> x0, local copies, waits for them, and re-layouts: 33.9 us -> none  [the longest x32 24.6 us: body(): lax.scan(lin_advance, start_memory, inputs, unroll=8)]
    add x161 -> x0, other arithmetic: 28.5 us -> none  [the longest x128 18.3 us: lin_advance(): memory * decays[:, None, :] - along[:, :, None] * rate_vec[:, None, :]]
  transfers between devices with their start and end apart: 3 -> 3, of which waited for: 1 -> 3; matrix products, arithmetic and copies ran while one was open for 50% -> 1% of each run, Pallas kernels for 0% -> 8%
where the time goes in v1:
time: 187 us; the launch traced here: 186 us
  blocking collectives  88 us (47%)
  Pallas kernels  47.2 us (25%)
  waiting for transfers between devices  20 us (11%)
  between operations  13.6 us (7%)
  starting transfers between devices  8.77 us (5%)
  local copies, waits for them, and re-layouts  7.54 us (4%)
    all_to_all x2, blocking collectives, sent_to_all(): lax.all_to_all(jnp.broadcast_to(a[None], (size, *a.shape)), axis, 0, 0, t...  67.8 us
    pallas_call x6, Pallas kernels, run(): pl.pallas_call(kernel, name=name, out_shape=shapes, in_specs=[smem()] * s...  47.2 us
    all_to_all x1, blocking collectives, body(): tiles = lax.all_to_all(partial, TP, 0, 0, tiled=True)  20.2 us
    all_to_all x1, waiting for transfers between devices, sent_to_all(): lax.all_to_all(jnp.broadcast_to(a[None], (size, *a.shape)), axis, 0, 0, t...  7.8 us
    all_gather x1, waiting for transfers between devices, body(): keys = lax.all_gather(kv, 'z', axis=0, tiled=True)  7.79 us
    unnamed x41, local copies, waits for them, and re-layouts  5.6 us
    all_to_all x1, starting transfers between devices, sent_to_all(): lax.all_to_all(jnp.broadcast_to(a[None], (size, *a.shape)), axis, 0, 0, t...  4.47 us
    all_to_all x1, waiting for transfers between devices, body(): parts = lax.all_to_all(found, 'y', 0, 0, tiled=True)  4.42 us
  transfers between devices with their start and end apart: 3, of which 3 were waited for; matrix products, arithmetic and copies ran while one was open for 1% of the time, Pallas kernels for 8%

profile of v1, /device:TPU:480, one launch (start us, length us, event | category | flops | bytes accessed | tf_op | source)
XLA Modules:
  0.0 186.0 jit_solution(11504008585147736280)
XLA Ops:
  6.5 0.0 copy-start.4
  6.5 0.0 all-gather.2.cloned.1.call-start
  6.5 1.1 broadcast_in_dim.6
  7.6 20.1 %all_to_all.25.pieces_ref = bf16[8,256,256]{2,1,0:T(8,128)(2,1)S(1)} all-to-all(bf16[8,256,256]{2,1,0:T(8,128)(2,1)S(1)} %broadcast_in_dim.6), channel_id=1, replica_groups=mesh['z'=16,'y'=4,'x'=4,'c'=2] {'x','c'}, dimensions={0} | all-to-all | bytes 2097152 | tf_op jit(solution)/shard_map/all_to_all | solution.py:368
  27.7 0.0 copy-start.14
  27.7 0.0 copy-start.15
  27.7 0.0 copy-start.16
  27.7 0.0 copy-done.4
  27.7 0.0 copy-done
  27.7 0.0 copy-done.1
  27.8 1.4 kv.1
  29.2 0.0 all-gather.2.cloned.1.call-update
  29.2 1.2 copy.20.down_ref
  30.4 0.0 copy-done.7
  30.4 0.0 copy-done.8
  30.4 0.0 copy-done.11
  30.5 0.0 copy-done.13
  30.5 0.0 copy-done.14
  30.5 0.0 copy-done.15
  30.5 0.0 copy-done.16
  30.5 0.0 copy-start.9
  30.5 1.0 copy-done.9
  31.5 1.0 copy-done.10
  32.6 10.8 %lin.1 = (bf16[400,128]{1,0:T(8,128)(2,1)S(1)}, bf16[16,128]{1,0:T(8,128)(2,1)S(1)}, f32[256,128]{1,0:T(8,128)S(1)}, f32[256,128]{1,0:T(8,128)S(1)}) custom-call(bf16[8,256,256]{2,1,0:T(8,128)(2,1)S(1)} %all_to_all.25.pieces_ref, f32[1,2048]{1,0:T(1,128)S(1)} %bitcast.9, bf16[2048,128]{1,0:T(8,128)(2,1)S(1)} %copy-done.7, bf16[2048,128]{1,0:T(8,128)(2,1)S(1)} %copy-done.8, ...), custom_call_target="tpu_custom_call" | custom-call | flops 4000000000 | bytes 4194304 | tf_op jit(solution)/shard_map/lin/pallas_call | solution.py:382
  43.4 0.0 copy-start.18
  43.4 0.6 copy-done.18
  44.0 0.8 broadcast_in_dim.7
  44.8 4.5 %all-to-all-start.1 = ((bf16[4,400,128]{2,1,0:T(8,128)(2,1)}), bf16[4,400,128]{2,1,0:T(8,128)(2,1)S(1)}, u32[]{:S(2)}, u32[]{:S(2)}) async-start(bf16[4,400,128]{2,1,0:T(8,128)(2,1)} %broadcast_in_dim.7), calls=%async_computation.1 | async-start | bytes 819200 | tf_op jit(solution)/shard_map/all_to_all | solution.py:368
  49.3 0.1 pad_add_fusion.place_ref
  49.4 7.8 %all-to-all-done.1.gathered_ref.asked_ref = bf16[4,400,128]{2,1,0:T(8,128)(2,1)S(1)} async-done(((bf16[4,400,128]{2,1,0:T(8,128)(2,1)}), bf16[4,400,128]{2,1,0:T(8,128)(2,1)S(1)}, u32[]{:S(2)}, u32[]{:S(2)}) %all-to-all-start.1) | async-done | bytes 409632 | tf_op jit(solution)/shard_map/all_to_all | solution.py:368
  57.2 1.1 row.1
  58.3 0.1 broadcast_in_dim.8
  58.4 47.7 %all_to_all.26.held_ref.gathered_ref = bf16[16,144,128]{2,1,0:T(8,128)(2,1)S(1)} all-to-all(bf16[16,144,128]{2,1,0:T(8,128)(2,1)S(1)} %broadcast_in_dim.8), channel_id=1, replica_groups=mesh['z'=16,'y'=4,'x'=4,'c'=2] {'z'}, dimensions={0} | all-to-all | bytes 1179648 | tf_op jit(solution)/shard_map/all_to_all | solution.py:368
  106.1 7.8 %all-gather.2.cloned.1.call-done.keys_ref = bf16[4096,256]{1,0:T(8,128)(2,1)} async-done(((bf16[256,256]{1,0:T(8,128)(2,1)}), bf16[4096,256]{1,0:T(8,128)(2,1)}) %all-gather.2.cloned.1.call-update) | async-done | bytes 2097168 | tf_op jit(solution)/shard_map/all_gather | solution.py:429
  113.9 1.6 copy-done.6
  115.5 29.1 %att.1 = bf16[4,256,256]{2,1,0:T(8,128)(2,1)} custom-call(s32[2]{0:T(128)S(1)} %pad_add_fusion.place_ref, bf16[4,400,128]{2,1,0:T(8,128)(2,1)S(1)} %all-to-all-done.1.gathered_ref.asked_ref, bf16[16,144,128]{2,1,0:T(8,128)(2,1)S(1)} %all_to_all.26.held_ref.gathered_ref, bf16[4096,256]{1,0:T(8,128)(2,1)S(1)} %copy-done.6), custom_call_target="tpu_custom_call" | custom-call | flops 2147483648 | bytes 4194304 | tf_op jit(solution)/shard_map/att/pallas_call | solution.py:382
  144.6 4.3 %all-to-all-start.3 = ((bf16[4,256,256]{2,1,0:T(8,128)(2,1)}), bf16[4,256,256]{2,1,0:T(8,128)(2,1)S(1)}, u32[]{:S(2)}, u32[]{:S(2)}) async-start(bf16[4,256,256]{2,1,0:T(8,128)(2,1)} %att.1), calls=%async_computation.3 | async-start | bytes 1048576 | tf_op jit(solution)/shard_map/all_to_all | solution.py:483
  148.9 0.0 copy-done.12
  148.9 0.0 copy-done.17
  148.9 0.0 copy-done.19
  148.9 3.6 %mix.1.lin_ref = bf16[256,128]{1,0:T(8,128)(2,1)S(1)} custom-call(s32[2]{0:T(128)S(1)} %pad_add_fusion.place_ref, f32[2,64,64]{2,1,0:T(8,128)S(1)} %copy-done.12, bf16[16,144,128]{2,1,0:T(8,128)(2,1)S(1)} %all_to_all.26.held_ref.gathered_ref, f32[2,128,128]{2,1,0:T(8,128)S(1)} %get-tuple-element.14.before_ref, f32[256,128]{1,0:T(8,128)S(1)} %get-tuple-element.15.reach_ref, ...), custom_call_target="tpu_custom_call" | custom-call | flops 1000000000 | bytes 1048576 | tf_op jit(solution)/shard_map/mix/pallas_call | solution.py:382
  152.6 4.4 %all-to-all-done.3.parts_ref = bf16[4,256,256]{2,1,0:T(8,128)(2,1)S(1)} async-done(((bf16[4,256,256]{2,1,0:T(8,128)(2,1)}), bf16[4,256,256]{2,1,0:T(8,128)(2,1)S(1)}, u32[]{:S(2)}, u32[]{:S(2)}) %all-to-all-start.3) | async-done | bytes 524320 | tf_op jit(solution)/shard_map/all_to_all | solution.py:483
  157.0 0.0 copy-done.2
  157.0 0.0 copy-done.3
  157.0 0.0 copy-done.5
  157.0 1.2 out.1
  158.2 20.2 %all_to_all.27 = bf16[8,256,256]{2,1,0:T(8,128)(2,1)S(1)} all-to-all(bf16[8,256,256]{2,1,0:T(8,128)(2,1)S(1)} %out.1), channel_id=1, replica_groups=mesh['z'=16,'y'=4,'x'=4,'c'=2] {'x','c'}, dimensions={0} | all-to-all | bytes 2097152 | tf_op jit(solution)/shard_map/all_to_all | solution.py:488
  178.4 0.8 reduce_sum.12
  (14 shorter events, 0.0 us)
Async XLA Ops:
  6.5 21.2 %copy-start.4 = (f32[2048]{0:T(1024)S(1)}, f32[2048]{0:T(1024)}, u32[]{:S(2)}) copy-start(f32[2048]{0:T(1024)} %param.20) | copy-start | bytes 24580
  6.5 21.2 %copy-start = (bf16[2048,128]{1,0:T(8,128)(2,1)S(1)}, bf16[2048,128]{1,0:T(8,128)(2,1)}, u32[]{:S(2)}) copy-start(bf16[2048,128]{1,0:T(8,128)(2,1)} %wk_ref.3) | copy-start | bytes 1572868
  6.5 21.2 %copy-start.1 = (bf16[2048,128]{1,0:T(8,128)(2,1)S(1)}, bf16[2048,128]{1,0:T(8,128)(2,1)}, u32[]{:S(2)}) copy-start(bf16[2048,128]{1,0:T(8,128)(2,1)} %wv_ref.3) | copy-start | bytes 1572868
  6.5 107.4 %all-gather.2.cloned.1.call-start = ((), (), s32[]{:S(2)}) async-start(), calls=%async_computation.5 | async-start | bytes 2228224 | tf_op jit(solution)/shard_map/all_gather | solution.py:429
  27.7 2.7 %copy-start.7 = (bf16[2048,128]{1,0:T(8,128)(2,1)S(1)}, bf16[2048,128]{1,0:T(8,128)(2,1)}, u32[]{:S(2)}) copy-start(bf16[2048,128]{1,0:T(8,128)(2,1)} %wr_ref.1) | copy-start | bytes 1572868
  27.7 2.8 %copy-start.8 = (bf16[2048,128]{1,0:T(8,128)(2,1)S(1)}, bf16[2048,128]{1,0:T(8,128)(2,1)}, u32[]{:S(2)}) copy-start(bf16[2048,128]{1,0:T(8,128)(2,1)} %wk_ref.2) | copy-start | bytes 1572868
  27.7 2.8 %copy-start.11 = (f32[256,128]{1,0:T(8,128)S(1)}, f32[256,128]{1,0:T(8,128)}, u32[]{:S(2)}) copy-start(f32[256,128]{1,0:T(8,128)} %shift_ref.1) | copy-start | bytes 393220
  27.7 2.8 %copy-start.13 = (bf16[64,128]{1,0:T(8,128)(2,1)S(1)}, bf16[64,128]{1,0:T(8,128)(2,1)}, u32[]{:S(2)}) copy-start(bf16[64,128]{1,0:T(8,128)(2,1)} %up_ref.1) | copy-start | bytes 49156
  27.7 2.8 %copy-start.14 = (f32[256,1]{0,1:T(1,128)S(1)}, f32[256,1]{0,1:T(1,128)}, u32[]{:S(2)}) copy-start(f32[256,1]{0,1:T(1,128)} %param.34) | copy-start | bytes 3076
  27.7 2.8 %copy-start.15 = (f32[128]{0:T(128)S(1)}, f32[128]{0:T(128)}, u32[]{:S(2)}) copy-start(f32[128]{0:T(128)} %param.26) | copy-start | bytes 1540
  27.7 2.8 %copy-start.16 = (f32[128]{0:T(128)S(1)}, f32[128]{0:T(128)}, u32[]{:S(2)}) copy-start(f32[128]{0:T(128)} %param.28) | copy-start | bytes 1540
  30.5 1.0 copy-start.9
  31.5 1.0 copy-start.10
  43.4 0.7 copy-start.18
  44.8 12.3 %all-to-all-start.1 = ((bf16[4,400,128]{2,1,0:T(8,128)(2,1)}), bf16[4,400,128]{2,1,0:T(8,128)(2,1)S(1)}, u32[]{:S(2)}, u32[]{:S(2)}) async-start(bf16[4,400,128]{2,1,0:T(8,128)(2,1)} %broadcast_in_dim.7), calls=%async_computation.1 | async-start | bytes 819200 | tf_op jit(solution)/shard_map/all_to_all | solution.py:368
  113.9 1.6 copy-start.6
  115.5 33.4 %copy-start.12 = (f32[2,64,64]{2,1,0:T(8,128)S(1)}, f32[2,64,64]{2,1,0:T(8,128)}, u32[]{:S(2)}) copy-start(f32[2,64,64]{2,1,0:T(8,128)} %state_ref.1) | copy-start | bytes 98308
  115.5 33.4 %copy-start.17 = (f32[128]{0:T(128)S(1)}, f32[128]{0:T(128)}, u32[]{:S(2)}) copy-start(f32[128]{0:T(128)} %param.29) | copy-start | bytes 1540
  115.5 33.4 %copy-start.19 = (f32[256,128]{1,0:T(8,128)S(1)}, f32[256,128]{1,0:T(8,128)}, u32[]{:S(2)}) copy-start(f32[256,128]{1,0:T(8,128)} %copy-done.18) | copy-start | bytes 393220
  144.6 12.4 %all-to-all-start.3 = ((bf16[4,256,256]{2,1,0:T(8,128)(2,1)}), bf16[4,256,256]{2,1,0:T(8,128)(2,1)S(1)}, u32[]{:S(2)}, u32[]{:S(2)}) async-start(bf16[4,256,256]{2,1,0:T(8,128)(2,1)} %att.1), calls=%async_computation.3 | async-start | bytes 1048576 | tf_op jit(solution)/shard_map/all_to_all | solution.py:483
  148.9 8.1 %copy-start.2 = (bf16[128,2048]{1,0:T(8,128)(2,1)S(1)}, bf16[128,2048]{1,0:T(8,128)(2,1)}, u32[]{:S(2)}) copy-start(bf16[128,2048]{1,0:T(8,128)(2,1)} %wl_ref.1) | copy-start | bytes 1572868
  148.9 8.1 %copy-start.3 = (bf16[128,2048]{1,0:T(8,128)(2,1)S(1)}, bf16[128,2048]{1,0:T(8,128)(2,1)}, u32[]{:S(2)}) copy-start(bf16[128,2048]{1,0:T(8,128)(2,1)} %wa_ref.1) | copy-start | bytes 1572868
  148.9 8.1 %copy-start.5 = (f32[128]{0:T(128)S(1)}, f32[128]{0:T(128)}, u32[]{:S(2)}) copy-start(f32[128]{0:T(128)} %param.35) | copy-start | bytes 1540
Sparse Core Ops, SparseCore 0:
  29.3 84.5 all-gather.1

commit v2 on v1

--- a/solution.py
+++ b/solution.py
@@ -20,8 +20,8 @@
 BF16 = jnp.bfloat16
 
 
-def params():
-    return pltpu.CompilerParams(vmem_limit_bytes=48 * 1024 * 1024)
+def params(mib):
+    return pltpu.CompilerParams(vmem_limit_bytes=mib * 1024 * 1024)
 
 
 def cost(flops, size):
@@ -59,29 +59,36 @@
     return jnp.where(left, first, second)
 
 
-def scaled_pieces(pieces_ref, gain_ref):
-    shards, rows, depth = pieces_ref.shape
+def scaled_pieces(place_ref, own_ref, other_ref, gain_ref):
+    shards, rows, depth = own_ref.shape
+    core = place_ref[2]
     scaled, squares = [], jnp.zeros((rows, depth), F32)
-    for j in range(shards):
-        wide = pieces_ref[j].astype(F32)
-        scaled.append((wide * gain_ref[:, j * depth : (j + 1) * depth]).astype(BF16))
-        squares = squares + wide * wide
-    mean = jnp.sum(squares, axis=1, keepdims=True) / (shards * depth)
+    for c, ref in enumerate((own_ref, other_ref)):
+        for j in range(shards):
+            start = pl.multiple_of((2 * j + (core if c == 0 else 1 - core)) * depth, depth)
+            wide = ref[j].astype(F32)
+            scaled.append(((wide * gain_ref[:, pl.ds(start, depth)]).astype(BF16), start))
+            squares = squares + wide * wide
+    mean = jnp.sum(squares, axis=1, keepdims=True) / (2 * shards * depth)
     return scaled, lax.rsqrt(mean + 1e-6)
 
 
 def projected(scaled, inverse, w_ref):
-    depth = scaled[0].shape[1]
-    total = dot(scaled[0], w_ref[0:depth])
-    for j in range(1, len(scaled)):
-        total = total + dot(scaled[j], w_ref[j * depth : (j + 1) * depth])
-    return (total * inverse).astype(BF16)
-
-
-def kv_kernel(pieces_ref, gain_ref, wk_ref, wv_ref, out_ref):
-    scaled, inverse = scaled_pieces(pieces_ref, gain_ref)
-    out_ref[:, :HEAD_ATT] = projected(scaled, inverse, wk_ref)
-    out_ref[:, HEAD_ATT:] = projected(scaled, inverse, wv_ref)
+    total = 0.0
+    for piece, start in scaled:
+        total = total + dot(piece, w_ref[pl.ds(start, piece.shape[1])])
+    return total * inverse
+
+
+def stacked(a):
+    return jnp.concatenate([a[:, :WIDE], a[:, WIDE:]], axis=0)
+
+
+def kv_kernel(place_ref, own_ref, other_ref, gain_ref, wk_ref, wv_ref, out_ref):
+    scaled, inverse = scaled_pieces(place_ref, own_ref, other_ref, gain_ref)
+    rows = own_ref.shape[1]
+    out_ref[0:rows] = projected(scaled, inverse, wk_ref).astype(BF16)
+    out_ref[rows:] = stacked(projected(scaled, inverse, wv_ref).T.astype(BF16))
 
 
 def spans(log_decay):
@@ -113,7 +120,9 @@
 
 
 def lin_kernel(
-    pieces_ref,
+    place_ref,
+    own_ref,
+    other_ref,
     gain_ref,
     wr_ref,
     wk_ref,
@@ -131,73 +140,92 @@
     local_ref,
     pairs_ref,
 ):
-    scaled, inverse = scaled_pieces(pieces_ref, gain_ref)
+    scaled, inverse = scaled_pieces(place_ref, own_ref, other_ref, gain_ref)
     rows = shift_ref.shape[0]
-    send_ref[0:rows] = projected(scaled, inverse, wq_ref)
-    recv = projected(scaled, inverse, wr_ref).astype(F32)
-    key = projected(scaled, inverse, wk_ref).astype(F32)
-    value = projected(scaled, inverse, wv_ref)
-    low = projected(scaled, inverse, down_ref).astype(F32)
+    send_ref[0:rows] = stacked(projected(scaled, inverse, wq_ref).T.astype(BF16))
+    recv = projected(scaled, inverse, wr_ref).astype(BF16).astype(F32)
+    key = projected(scaled, inverse, wk_ref).astype(BF16).astype(F32)
+    value = projected(scaled, inverse, wv_ref).astype(BF16)
+    low = 0.0
+    for piece, start in scaled:
+        low = low + dot(piece, down_ref[:, pl.ds(start, piece.shape[1])], ((1,), (1,)))
+    low = (low * inverse).astype(BF16).astype(F32)
     exponent = bias_ref[...] + shift_ref[...] + dot(jnp.tanh(low).astype(BF16), up_ref[...])
     log_decay = -jnp.exp(exponent)
     unit = key * lax.rsqrt(by_head(key * key) + 1e-6)
     rate = unit * rate_ref[...]
 
     ahead, after = spans(log_decay)
+    half = rows // 2
     lane = iota((rows, WIDE), 1)
     row = iota((rows, WIDE), 0)
-    tall = iota((rows, rows), 0)
-    flat = iota((rows, rows), 1)
+    tall = iota((half, half), 0)
+    flat = iota((half, half), 1)
     heads = [lane < HEAD_LIN, lane >= HEAD_LIN]
+    eye = tall == flat
+    blocks = slice(0, half), slice(half, rows)
 
     def of_heads(a):
         return [jnp.where(mine, a, 0.0).astype(BF16) for mine in heads]
 
-    eye = tall == flat
-    right_now = jnp.concatenate([key, rate], axis=0).astype(BF16)
-    for n, q_part in enumerate(of_heads(recv)):
-        product = dot(q_part, right_now, ((1,), (1,)))
-        for m in range(2):
-            mine = slice(m * rows, (m + 1) * rows)
-            pairs_ref[n, 1, :, mine] = jnp.where(eye, product[:, mine], 0.0)
-            pairs_ref[n, 0, :, mine] = jnp.zeros((rows, rows), F32)
-    h, level = 1, 0
+    def below(h):
+        level = h.bit_length()
+        near = (tall >> level) == (flat >> level)
+        return near & ((tall & h) != 0) & ((flat & h) == 0)
+
+    for m, source in enumerate((key, rate)):
+        now = by_head(recv * source)
+        for n in range(2):
+            for b in range(2):
+                cols = slice(m * rows + b * half, m * rows + (b + 1) * half)
+                same_row = now[blocks[b], n * HEAD_LIN : n * HEAD_LIN + 1]
+                pairs_ref[n, 1, blocks[b], cols] = jnp.where(eye, same_row, 0.0)
+                pairs_ref[n, 0, blocks[b], cols] = jnp.zeros((half, half), F32)
+            cols = slice(m * rows + half, (m + 1) * rows)
+            for k in range(2):
+                pairs_ref[n, k, blocks[0], cols] = jnp.zeros((half, half), F32)
+    h = 1
     while h < rows:
         late = (row & h) != 0
         to_u = jnp.where(late, jnp.exp(ahead[h]), 0.0)
         to_q = jnp.where(late, jnp.exp(ahead[h] + log_decay), 0.0)
         from_s = jnp.where(late, 0.0, jnp.exp(after[h]))
-        right = jnp.concatenate([key * from_s, rate * from_s], axis=0).astype(BF16)
-        left = of_heads(unit * to_u), of_heads(recv * to_q)
-        here = ((tall >> (level + 1)) == (flat >> (level + 1))) & ((tall & h) != 0) & (
-            (flat & h) == 0
-        )
+        right = (key * from_s).astype(BF16), (rate * from_s).astype(BF16)
+        left = of_heads(unit * to_u) + of_heads(recv * to_q)
+        for b in range(2) if h < half else (1,):
+            c = b if h < half else 0
+            product = dot(
+                jnp.concatenate([a[blocks[b]] for a in left], axis=0),
+                jnp.concatenate([a[blocks[c]] for a in right], axis=0),
+                ((1,), (1,)),
+            )
+            for k in range(2):
+                for n in range(2):
+                    for m in range(2):
+                        cols = slice(m * rows + c * half, m * rows + (c + 1) * half)
+                        new = product[
+                            (2 * k + n) * half : (2 * k + n + 1) * half,
+                            m * half : (m + 1) * half,
+                        ]
+                        if h < half:
+                            new = jnp.where(below(h), new, pairs_ref[n, k, blocks[b], cols])
+                        pairs_ref[n, k, blocks[b], cols] = new
+        h *= 2
+
+    solved = {}
+    h = 1
+    while h < half:
+        here = below(h)
         for n in range(2):
-            for k in range(2):
-                product = dot(left[k][n], right, ((1,), (1,)))
-                for m in range(2):
-                    mine = slice(m * rows, (m + 1) * rows)
-                    pairs_ref[n, k, :, mine] = jnp.where(
-                        here, product[:, mine], pairs_ref[n, k, :, mine]
-                    )
+            for b in range(2):
+                cols = slice(rows + b * half, rows + (b + 1) * half)
+                links = jnp.where(here, pairs_ref[n, 0, blocks[b], cols], 0.0)
+                if h == 1:
+                    solved[n, b] = jnp.where(eye, 1.0, 0.0) - links
+                else:
+                    step = dot3(links, solved[n, b])
+                    solved[n, b] = solved[n, b] - dot3(solved[n, b], step)
         h *= 2
-        level += 1
-
-    solved = [jnp.where(eye, 1.0, 0.0) for _ in range(2)]
-    h, level = 1, 0
-    while h < rows:
-        here = ((tall >> (level + 1)) == (flat >> (level + 1))) & ((tall & h) != 0) & (
-            (flat & h) == 0
-        )
-        for n in range(2):
-            links = jnp.where(here, pairs_ref[n, 0, :, rows:], 0.0)
-            if h == 1:
-                solved[n] = solved[n] - links
-            else:
-                step = dot3(links, solved[n])
-                solved[n] = solved[n] - dot3(solved[n], step)
-        h *= 2
-        level += 1
 
     full_u = unit * jnp.exp(ahead[rows])
     full_q = recv * jnp.exp(ahead[rows] + log_decay)
@@ -208,7 +236,9 @@
     for n in range(2):
         add = dot2(pairs_ref[n, 0, :, :rows], value)
         source = jnp.where(heads[n], full_u, pltpu.roll(add, HEAD_LIN, 1))
-        along = dot3(solved[n], source)
+        first = dot3(solved[n, 0], source[:half])
+        later = source[half:] - dot3(pairs_ref[n, 0, half:, rows : rows + half], first)
+        along = jnp.concatenate([first, dot3(solved[n, 1], later)], axis=0)
         taken = dot3(pairs_ref[n, 1, :, rows:], along)
         reach.append(full_q - taken)
         local.append(dot2(pairs_ref[n, 1, :, :rows], value) - pltpu.roll(taken, HEAD_LIN, 1))
@@ -296,71 +326,87 @@
     return gates[0:2] + gates[2:4] + gates[4:6]
 
 
-def att_kernel(place_ref, asked_ref, held_ref, keys_ref, out_ref, best_ref, sum_ref, *, rows):
+def att_kernel(
+    place_ref, asked_ref, held_ref, keys_ref, out_ref, best_ref, sum_ref, block_ref, sems, *, rows
+):
     z, y = place_ref[0], place_ref[1]
     count = asked_ref.shape[0]
     scale = HEAD_ATT ** (-0.5) * LOG2E
+
+    def fetch(k):
+        start = pl.multiple_of(k * 2 * rows, 2 * rows)
+        return pltpu.make_async_copy(
+            keys_ref.at[pl.ds(start, 2 * rows)], block_ref.at[k], sems.at[k]
+        )
+
+    lax.fori_loop(0, z + 1, lambda k, c: (fetch(k).start(), c)[1], 0)
     best_ref[...] = jnp.full(best_ref.shape, NEG, F32)
     sum_ref[...] = jnp.zeros(sum_ref.shape, F32)
-    ones = jnp.ones((rows, HEAD_ATT), BF16)
-    zero_gate = [joined(asked_ref[j, rows + WIDE : rows + WIDE + 16])[0:1, 0:1] for j in range(count)]
+    ones = jnp.ones((16, rows), BF16)
+    base = joined(asked_ref[0, rows + WIDE : rows + WIDE + 16])[0:1, 0:1]
 
     def block(k, masked):
-        start = pl.multiple_of(k * rows, rows)
-        both = keys_ref[pl.ds(start, rows)]
-        key = both[:, :HEAD_ATT]
-        value = jnp.concatenate([both[:, HEAD_ATT:], ones], axis=1)
-        gate = joined(held_ref[k][WIDE : WIDE + 16])
-        gate = jnp.concatenate([gate[0:1], gate[1:2]], axis=1)
+        fetch(k).wait()
+        key = block_ref[k, 0:rows]
+        left, right = block_ref[k, rows : rows + WIDE], block_ref[k, rows + WIDE :]
+        value = jnp.concatenate([jnp.concatenate([left, right], axis=1), ones], axis=0)
+        drop = (base - joined(held_ref[k, WIDE : WIDE + 16])) * LOG2E
+        drop = [jnp.broadcast_to(drop[i : i + 1], (WIDE, WIDE)).T for i in range(2)]
+        drop = jnp.concatenate(drop, axis=0)
+        drop = jnp.concatenate([drop, drop], axis=1)
         for j in range(count):
-            logits = dot(asked_ref[j, 0:rows], key, ((1,), (1,))) * scale
-            logits = logits + (zero_gate[j] - gate) * LOG2E
+            asked = jnp.concatenate([asked_ref[j, 0:WIDE], asked_ref[j, WIDE:rows]], axis=1)
+            logits = dot(key, asked) * scale + drop
             if masked:
-                allowed = y * rows + iota(logits.shape, 1) <= j * rows + iota(logits.shape, 0)
+                allowed = y * rows + iota(logits.shape, 0) <= j * rows + iota(logits.shape, 1)
                 logits = jnp.where(allowed, logits, NEG)
-            old = best_ref[j][:, 0:1]
-            new = jnp.maximum(old, jnp.max(logits, axis=1, keepdims=True))
+            old = best_ref[j]
+            new = jnp.maximum(old, jnp.max(logits, axis=0, keepdims=True))
             weights = jnp.exp2(logits - new)
             if masked:
                 weights = jnp.where(allowed, weights, 0.0)
-            sum_ref[j] = sum_ref[j] * jnp.exp2(old - new) + dot(weights.astype(BF16), value)
-            best_ref[j] = jnp.broadcast_to(new, (rows, WIDE))
+            sum_ref[j] = sum_ref[j] * jnp.exp2(old - new) + dot(value, weights.astype(BF16))
+            best_ref[j] = new
 
     lax.fori_loop(0, z, lambda k, c: (block(k, False), c)[1], 0)
     block(z, True)
-    third = iota((rows, WIDE), 1)
+    third = iota((16, rows), 0)
     for j in range(count):
-        total = sum_ref[j][:, HEAD_ATT:]
+        total = sum_ref[j, HEAD_ATT : HEAD_ATT + 1]
         some = total > 0.0
         safe = jnp.where(some, total, 1.0)
-        out_ref[j, :, :HEAD_ATT] = (sum_ref[j][:, :HEAD_ATT] / safe).astype(BF16)
+        out_ref[j, 0:HEAD_ATT] = (sum_ref[j, 0:HEAD_ATT] / safe).astype(BF16)
         level = jnp.where(some, best_ref[j] + jnp.log(safe) * LOG2E, NEG)
         high, mid = parts_of(level)
-        last = (level - high.astype(F32) - mid.astype(F32)).astype(BF16)
-        level = jnp.where(third < 40, high.astype(F32), jnp.where(third < 80, mid.astype(F32), last.astype(F32)))
-        out_ref[j, :, HEAD_ATT:] = level.astype(BF16)
-
-
-def out_kernel(parts_ref, lin_ref, gain_ref, wl_ref, wa_ref, out_ref):
-    count, rows = parts_ref.shape[0], parts_ref.shape[1]
+        high, mid = high.astype(F32), mid.astype(F32)
+        last = level - high - mid
+        level = jnp.where(third == 0, high, jnp.where(third == 1, mid, last))
+        out_ref[j, HEAD_ATT:] = level.astype(BF16)
+
+
+def out_kernel(place_ref, parts_ref, lin_ref, gain_ref, wl_ref, wa_ref, own_ref, other_ref):
+    count, rows = parts_ref.shape[0], parts_ref.shape[2]
+    core = place_ref[2]
     levels = []
     for j in range(count):
-        level = parts_ref[j, :, HEAD_ATT:].astype(F32)
-        levels.append(level[:, 0:1] + level[:, 40:41] + level[:, 80:81])
+        level = parts_ref[j, HEAD_ATT:].astype(F32)
+        levels.append(level[0:1] + level[1:2] + level[2:3])
     top = functools.reduce(jnp.maximum, levels)
-    total, raw = jnp.zeros((rows, 1), F32), jnp.zeros((rows, HEAD_ATT), F32)
+    total, raw = jnp.zeros((1, rows), F32), jnp.zeros((HEAD_ATT, rows), F32)
     for j in range(count):
         share = jnp.exp2(levels[j] - top)
         total = total + share
-        raw = raw + share * parts_ref[j, :, :HEAD_ATT].astype(F32)
+        raw = raw + share * parts_ref[j, 0:HEAD_ATT].astype(F32)
     raw = raw / total
-    size = jnp.mean(raw * raw, axis=1, keepdims=True)
-    att = (raw * lax.rsqrt(size + 1e-6) * gain_ref[...]).astype(BF16)
+    size = jnp.mean(raw * raw, axis=0, keepdims=True)
+    att = ((raw * lax.rsqrt(size + 1e-6)).T * gain_ref[...]).astype(BF16)
     lin = lin_ref[...]
-    width = out_ref.shape[2]
-    for j in range(out_ref.shape[0]):
-        mine = slice(j * width, (j + 1) * width)
-        out_ref[j] = (dot(lin, wl_ref[:, mine]) + dot(att, wa_ref[:, mine])).astype(BF16)
+    width = own_ref.shape[2]
+    for c, ref in enumerate((own_ref, other_ref)):
+        for j in range(ref.shape[0]):
+            start = pl.multiple_of((2 * j + (core if c == 0 else 1 - core)) * width, width)
+            mine = pl.ds(start, width)
+            ref[j] = (dot(lin, wl_ref[:, mine]) + dot(att, wa_ref[:, mine])).astype(BF16)
 
 
 def sent_to_all(a, axis):
@@ -368,6 +414,10 @@
     return lax.all_to_all(jnp.broadcast_to(a[None], (size, *a.shape)), axis, 0, 0, tiled=True)
 
 
+def to_other_core(a):
+    return lax.ppermute(a, "c", [(0, 1), (1, 0)])
+
+
 def smem():
     return pl.BlockSpec(memory_space=pltpu.SMEM)
 
@@ -376,17 +426,22 @@
     return pl.BlockSpec(memory_space=pltpu.VMEM)
 
 
-def call(kernel, name, shapes, flops, size, scratch=(), scalars=0):
+def hbm():
+    return pl.BlockSpec(memory_space=pltpu.HBM)
+
+
+def call(kernel, name, shapes, flops, size, mib, scratch=(), outside=0):
     def run(*operands):
         many = isinstance(shapes, (list, tuple))
+        inside = len(operands) - 1 - outside
         return pl.pallas_call(
             kernel,
             name=name,
             out_shape=shapes,
-            in_specs=[smem()] * scalars + [vmem()] * (len(operands) - scalars),
+            in_specs=[smem()] + [vmem()] * inside + [hbm()] * outside,
             out_specs=[vmem()] * len(shapes) if many else vmem(),
             scratch_shapes=list(scratch),
-            compiler_params=params(),
+            compiler_params=params(mib),
             cost_estimate=cost(flops, size),
         )(*operands)
 
@@ -415,17 +470,17 @@
     out_att_weight,
 ):
     rows = tokens.shape[0]
-    nz, ny = lax.axis_size("z"), lax.axis_size("y")
-    ntp = lax.axis_size(TP)
+    nz, ny, nx = (lax.axis_size(axis) for axis in ("z", "y", "x"))
     model_width = norm_gain.shape[0]
     shape = jax.ShapeDtypeStruct
-    place = jnp.stack([lax.axis_index("z"), lax.axis_index("y")]).astype(jnp.int32)
+    place = jnp.stack([lax.axis_index(axis) for axis in ("z", "y", "c")]).astype(jnp.int32)
     gain = norm_gain.reshape(1, -1)
 
-    pieces = sent_to_all(tokens, TP)
-    kv = call(kv_kernel, "kv", shape((rows, 256), BF16), 2 * rows * model_width * 256, 1 << 21)(
-        pieces, gain, att_key_weight, att_value_weight
-    )
+    own = sent_to_all(tokens, "x")
+    other = to_other_core(own)
+    kv = call(
+        kv_kernel, "kv", shape((2 * rows, WIDE), BF16), 2 * rows * model_width * 256, 1 << 21, 12
+    )(place, own, other, gain, att_key_weight, att_value_weight)
     keys = lax.all_gather(kv, "z", axis=0, tiled=True)
 
     extra = 16
@@ -440,15 +495,18 @@
         ),
         4 * 10**9,
         1 << 22,
+        24,
         scratch=[pltpu.VMEM((2, 2, rows, 2 * rows), F32)],
     )(
-        pieces,
+        place,
+        own,
+        other,
         gain,
         recv_weight,
         lin_key_weight,
         lin_value_weight,
         query_weight,
-        decay_down,
+        decay_down.T,
         decay_up,
         decay_log_bias.reshape(1, -1),
         decay_shift,
@@ -462,30 +520,36 @@
         (shape((WIDE + extra, WIDE), BF16), shape((2, WIDE, WIDE), F32)),
         10**8,
         1 << 20,
-        scalars=1,
+        12,
     )(place, asked, gates)
-    held = sent_to_all(row_send, "z")
-    lin_mixed = call(
-        mix_kernel, "mix", shape((rows, WIDE), BF16), 10**9, 1 << 20, scalars=1
-    )(place, initial_state, held, before, reach, local, group_gain.reshape(1, -1))
+    held = lax.all_gather(row_send, "z")
+    lin_mixed = call(mix_kernel, "mix", shape((rows, WIDE), BF16), 10**9, 1 << 20, 12)(
+        place, initial_state, held, before, reach, local, group_gain.reshape(1, -1)
+    )
+    asked, lin_mixed = lax.optimization_barrier((asked, lin_mixed))
     found = call(
         functools.partial(att_kernel, rows=rows),
         "att",
-        shape((ny, rows, 256), BF16),
+        shape((ny, HEAD_ATT + 16, rows), BF16),
         ny * rows * nz * rows * 512,
         1 << 22,
+        24,
         scratch=[
-            pltpu.VMEM((ny, rows, WIDE), F32),
-            pltpu.VMEM((ny, rows, 256), F32),
+            pltpu.VMEM((ny, 1, rows), F32),
+            pltpu.VMEM((ny, HEAD_ATT + 16, rows), F32),
+            pltpu.VMEM((nz, 2 * rows, WIDE), BF16),
+            pltpu.SemaphoreType.DMA((nz,)),
         ],
-        scalars=1,
+        outside=1,
     )(place, asked, held, keys)
     parts = lax.all_to_all(found, "y", 0, 0, tiled=True)
-    width = model_width // ntp
-    partial = call(
-        out_kernel, "out", shape((ntp, rows, width), BF16), 2 * rows * 256 * model_width, 1 << 21
-    )(parts, lin_mixed, att_gain.reshape(1, -1), out_lin_weight, out_att_weight)
-    tiles = lax.all_to_all(partial, TP, 0, 0, tiled=True)
+    width = model_width // (2 * nx)
+    tile = shape((nx, rows, width), BF16)
+    mine, theirs = call(
+        out_kernel, "out", (tile, tile), 2 * rows * 256 * model_width, 1 << 21, 12
+    )(place, parts, lin_mixed, att_gain.reshape(1, -1), out_lin_weight, out_att_weight)
+    pair = (mine.astype(F32) + to_other_core(theirs).astype(F32)).astype(BF16)
+    tiles = lax.all_to_all(pair, "x", 0, 0, tiled=True)
     return jnp.sum(tiles.astype(F32), axis=0).astype(BF16)
 
 

time: 187 us -> 163 us (0.87)
  waiting for transfers between devices: 20 us -> 11.9 us
  Pallas kernels: 47.2 us -> 40.5 us
  starting transfers between devices: 8.77 us -> 3.87 us
  blocking collectives: 88 us -> 85.3 us
    all_to_all x2, blocking collectives: 67.8 us -> 26.4 us  [sent_to_all(): lax.all_to_all(jnp.broadcast_to(a[None], (size, *a.shape)), axis, 0, 0, t...]
    all_gather x0 -> x1, blocking collectives: none -> 34.4 us  [body(): held = lax.all_gather(row_send, 'z')]
    all_to_all x2 -> x0, waiting for transfers between devices: 12.2 us -> none  [the longest x1 7.8 us: sent_to_all(): lax.all_to_all(jnp.broadcast_to(a[None], (size, *a.shape)), axis, 0, 0, t...]
    all_to_all x2 -> x0, starting transfers between devices: 8.77 us -> none  [the longest x1 4.47 us: sent_to_all(): lax.all_to_all(jnp.broadcast_to(a[None], (size, *a.shape)), axis, 0, 0, t...]
    pallas_call x6, Pallas kernels: 47.2 us -> 40.5 us  [run(): pl.pallas_call(kernel, name=name, out_shape=shapes, in_specs=[smem()] + [...]
    all_to_all x1 -> x2, blocking collectives: 20.2 us -> 24.6 us  [the longest x1 14.1 us: body(): tiles = lax.all_to_all(pair, 'x', 0, 0, tiled=True)]
    ppermute x0 -> x2, starting transfers between devices: none -> 3.83 us  [to_other_core(): return lax.ppermute(a, 'c', [(0, 1), (1, 0)])]
    ppermute x0 -> x2, waiting for transfers between devices: none -> 3.67 us  [to_other_core(): return lax.ppermute(a, 'c', [(0, 1), (1, 0)])]
  transfers between devices with their start and end apart: 3 -> 3, of which waited for: 3 -> 3; matrix products, arithmetic and copies ran while one was open for 1% -> 0% of each run, Pallas kernels for 8% -> 8%
where the time goes in v2:
time: 163 us
  blocking collectives  85.3 us (52%)
  Pallas kernels  40.5 us (25%)
  between operations  13.6 us (8%)
  waiting for transfers between devices  11.9 us (7%)
  local copies, waits for them, and re-layouts  6.45 us (4%)
  starting transfers between devices  3.87 us (2%)
    pallas_call x6, Pallas kernels, run(): pl.pallas_call(kernel, name=name, out_shape=shapes, in_specs=[smem()] + [...  40.5 us
    all_gather x1, blocking collectives, body(): held = lax.all_gather(row_send, 'z')  34.4 us
    all_to_all x2, blocking collectives, sent_to_all(): lax.all_to_all(jnp.broadcast_to(a[None], (size, *a.shape)), axis, 0, 0, t...  26.4 us
    all_to_all x1, blocking collectives, body(): tiles = lax.all_to_all(pair, 'x', 0, 0, tiled=True)  14.1 us
    all_to_all x1, blocking collectives, body(): parts = lax.all_to_all(found, 'y', 0, 0, tiled=True)  10.5 us
    all_gather x1, waiting for transfers between devices, body(): keys = lax.all_gather(kv, 'z', axis=0, tiled=True)  8.18 us
    unnamed x40, local copies, waits for them, and re-layouts  5.34 us
    ppermute x2, starting transfers between devices, to_other_core(): return lax.ppermute(a, 'c', [(0, 1), (1, 0)])  3.83 us
  transfers between devices with their start and end apart: 3, of which 3 were waited for; matrix products, arithmetic and copies ran while one was open for 0% of the time, Pallas kernels for 8%

profile of v2, /device:TPU:480, one launch (start us, length us, event | category | flops | bytes accessed | tf_op | source)
XLA Modules:
  0.0 162.6 jit_solution(5735632661767181164)
XLA Ops:
  6.5 0.0 copy-start.9
  6.6 0.0 copy-start.10
  6.6 0.0 copy-start.15
  6.6 0.0 all-gather.3.cloned.1.call-start
  6.6 1.1 broadcast_in_dim.4
  7.7 13.6 %all_to_all.20.own_ref = bf16[4,256,256]{2,1,0:T(8,128)(2,1)S(1)} all-to-all(bf16[4,256,256]{2,1,0:T(8,128)(2,1)S(1)} %broadcast_in_dim.4), channel_id=1, replica_groups=mesh['z'=16,'y'=4,'x'=4,'c'=2] {'x'}, dimensions={0} | all-to-all | bytes 1048576 | tf_op jit(solution)/shard_map/all_to_all | solution.py:414
  21.3 1.9 %collective-permute-start = (bf16[4,256,256]{2,1,0:T(8,128)(2,1)S(1)}, bf16[4,256,256]{2,1,0:T(8,128)(2,1)S(1)}, u32[]{:S(2)}, u32[]{:S(2)}) collective-permute-start(bf16[4,256,256]{2,1,0:T(8,128)(2,1)S(1)} %all_to_all.20.own_ref), channel_id=1, source_target_pairs={{0,1},{1,0},{2,3},{3,2},{4,5},{5,4},{6,7},{7,6},{8,9},{9,8},{10,11... | collective-permute-start | bytes 1572872 | tf_op jit(solution)/shard_map/ppermute | solution.py:418
  23.2 0.1 pad_add_fusion.place_ref
  23.3 1.8 %collective-permute-done.other_ref = bf16[4,256,256]{2,1,0:T(8,128)(2,1)S(1)} collective-permute-done((bf16[4,256,256]{2,1,0:T(8,128)(2,1)S(1)}, bf16[4,256,256]{2,1,0:T(8,128)(2,1)S(1)}, u32[]{:S(2)}, u32[]{:S(2)}) %collective-permute-start) | collective-permute-done | bytes 524320 | tf_op jit(solution)/shard_map/ppermute | solution.py:418
  25.0 1.0 copy-done
  26.1 1.0 copy-done.1
  27.1 0.7 copy-done.4
  27.8 2.1 %kv.1 = bf16[512,128]{1,0:T(8,128)(2,1)} custom-call(s32[3]{0:T(128)S(1)} %pad_add_fusion.place_ref, bf16[4,256,256]{2,1,0:T(8,128)(2,1)S(1)} %all_to_all.20.own_ref, bf16[4,256,256]{2,1,0:T(8,128)(2,1)S(1)} %collective-permute-done.other_ref, f32[1,2048]{1,0:T(1,128)S(1)} %bitcast.13, bf16[2048,128]{1,0:T(8,128)(2,1)S(1)} %copy-done, ...), custom_call_target="tpu_custom_call" | custom-call | flops 268435456 | bytes 2097152 | tf_op jit(solution)/shard_map/kv/pallas_call | solution.py:437
  29.9 0.0 all-gather.3.cloned.1.call-update
  29.9 0.0 copy-done.5
  29.9 0.0 copy-done.17
  29.9 0.0 copy-done.18
  29.9 0.0 copy-done.16
  29.9 0.0 copy-done.8
  30.0 0.0 copy-done.9
  30.0 0.0 copy-done.10
  30.0 0.0 copy-done.15
  30.0 0.0 copy-done.11
  30.0 0.0 copy-done.12
  30.0 0.0 copy-start.13
  30.0 0.9 copy-done.13
  30.9 8.4 %lin.1 = (bf16[400,128]{1,0:T(8,128)(2,1)S(1)}, bf16[16,128]{1,0:T(8,128)(2,1)S(1)}, f32[256,128]{1,0:T(8,128)S(1)}, f32[256,128]{1,0:T(8,128)S(1)}) custom-call(s32[3]{0:T(128)S(1)} %pad_add_fusion.place_ref, bf16[4,256,256]{2,1,0:T(8,128)(2,1)S(1)} %all_to_all.20.own_ref, bf16[4,256,256]{2,1,0:T(8,128)(2,1)S(1)} %collective-permute-done.other_ref, ...), custom_call_target="tpu_custom_call" | custom-call | flops 4000000000 | bytes 4194304 | tf_op jit(solution)/shard_map/lin/pallas_call | solution.py:437
  39.3 0.0 copy-start.14
  39.3 0.0 copy-start.19
  39.3 0.1 broadcast_in_dim.5
  39.4 12.8 %all_to_all.21.gathered_ref.asked_ref = bf16[4,400,128]{2,1,0:T(8,128)(2,1)S(1)} all-to-all(bf16[4,400,128]{2,1,0:T(8,128)(2,1)S(1)} %broadcast_in_dim.5), channel_id=1, replica_groups=mesh['z'=16,'y'=4,'x'=4,'c'=2] {'y'}, dimensions={0} | all-to-all | bytes 819200 | tf_op jit(solution)/shard_map/all_to_all | solution.py:414
  52.2 1.1 row.1
  53.3 34.4 %all-gather = bf16[2304,128]{1,0:T(8,128)(2,1)S(1)} all-gather(bf16[144,128]{1,0:T(8,128)(2,1)S(1)} %get-tuple-element.17), channel_id=2, replica_groups=mesh['z'=16,'y'=4,'x'=4,'c'=2] {'z'}, dimensions={0}, use_global_device_ids=true | all-gather | bytes 626688 | tf_op jit(solution)/shard_map/all_gather | solution.py:525
  87.7 0.0 copy-done.14
  87.7 3.6 %mix.1.lin_ref = bf16[256,128]{1,0:T(8,128)(2,1)S(1)} custom-call(s32[3]{0:T(128)S(1)} %pad_add_fusion.place_ref, f32[2,64,64]{2,1,0:T(8,128)S(1)} %copy-done.14, bf16[16,144,128]{2,1,0:T(8,128)(2,1)S(1)} %bitcast.11, f32[2,128,128]{2,1,0:T(8,128)S(1)} %get-tuple-element.18.before_ref, f32[256,128]{1,0:T(8,128)S(1)} %get-tuple-element.19.reach_ref, ...), custom_call_target="tpu_custom_call" | custom-call | flops 1000000000 | bytes 1048576 | tf_op jit(solution)/shard_map/mix/pallas_call | solution.py:437
  91.3 0.0 copy-start.2
  91.3 0.0 copy-start.3
  91.3 0.0 copy-start.6
  91.3 8.2 %all-gather.3.cloned.1.call-done.keys_ref = bf16[8192,128]{1,0:T(8,128)(2,1)} async-done(((bf16[512,128]{1,0:T(8,128)(2,1)}), bf16[8192,128]{1,0:T(8,128)(2,1)}) %all-gather.3.cloned.1.call-update) | async-done | bytes 2097168 | tf_op jit(solution)/shard_map/all_gather | solution.py:484
  99.5 1.6 copy-done.7
  101.1 24.0 %att.1 = bf16[4,144,256]{2,1,0:T(8,128)(2,1)S(1)} custom-call(s32[3]{0:T(128)S(1)} %pad_add_fusion.place_ref, bf16[4,400,128]{2,1,0:T(8,128)(2,1)S(1)} %all_to_all.21.gathered_ref.asked_ref, bf16[16,144,128]{2,1,0:T(8,128)(2,1)S(1)} %bitcast.12, bf16[8192,128]{1,0:T(8,128)(2,1)S(1)} %copy-done.7), custom_call_target="tpu_custom_call" | custom-call | flops 2147483648 | bytes 4194304 | tf_op jit(solution)/shard_map/att/pallas_call | solution.py:437
  125.1 10.5 %all_to_all.22.parts_ref = bf16[4,144,256]{2,1,0:T(8,128)(2,1)S(1)} all-to-all(bf16[4,144,256]{2,1,0:T(8,128)(2,1)S(1)} %att.1), channel_id=1, replica_groups=mesh['z'=16,'y'=4,'x'=4,'c'=2] {'y'}, dimensions={0} | all-to-all | bytes 589824 | tf_op jit(solution)/shard_map/all_to_all | solution.py:545
  135.6 1.4 out.1
  137.0 1.9 %collective-permute-start.1 = (bf16[4,256,256]{2,1,0:T(8,128)(2,1)S(1)}, bf16[4,256,256]{2,1,0:T(8,128)(2,1)S(1)}, u32[]{:S(2)}, u32[]{:S(2)}) collective-permute-start(bf16[4,256,256]{2,1,0:T(8,128)(2,1)S(1)} %get-tuple-element.24), channel_id=1, source_target_pairs={{0,1},{1,0},{2,3},{3,2},{4,5},{5,4},{6,7},{7,6},{8,9},{9,8},{10,11... | collective-permute-start | bytes 1572872 | tf_op jit(solution)/shard_map/ppermute | solution.py:418
  138.9 1.9 %collective-permute-done.1 = bf16[4,256,256]{2,1,0:T(8,128)(2,1)S(1)} collective-permute-done((bf16[4,256,256]{2,1,0:T(8,128)(2,1)S(1)}, bf16[4,256,256]{2,1,0:T(8,128)(2,1)S(1)}, u32[]{:S(2)}, u32[]{:S(2)}) %collective-permute-start.1) | collective-permute-done | bytes 524320 | tf_op jit(solution)/shard_map/ppermute | solution.py:418
  140.8 0.1 add_convert_fusion
  140.9 14.1 %all_to_all.23 = bf16[4,256,256]{2,1,0:T(8,128)(2,1)S(1)} all-to-all(bf16[4,256,256]{2,1,0:T(8,128)(2,1)S(1)} %add_convert_fusion), channel_id=1, replica_groups=mesh['z'=16,'y'=4,'x'=4,'c'=2] {'x'}, dimensions={0} | all-to-all | bytes 1048576 | tf_op jit(solution)/shard_map/all_to_all | solution.py:552
  155.0 0.7 reduce_sum.12
  (15 shorter events, 0.0 us)
Async XLA Ops:
  6.5 23.4 %copy-start.5 = (f32[2048]{0:T(1024)S(1)}, f32[2048]{0:T(1024)}, u32[]{:S(2)}) copy-start(f32[2048]{0:T(1024)} %param.20) | copy-start | bytes 24580
  6.5 23.4 %copy-start.17 = (f32[128]{0:T(128)S(1)}, f32[128]{0:T(128)}, u32[]{:S(2)}) copy-start(f32[128]{0:T(128)} %param.26) | copy-start | bytes 1540
  6.5 23.4 %copy-start.18 = (f32[128]{0:T(128)S(1)}, f32[128]{0:T(128)}, u32[]{:S(2)}) copy-start(f32[128]{0:T(128)} %param.28) | copy-start | bytes 1540
  6.5 23.4 %copy-start.16 = (f32[256,1]{0,1:T(1,128)S(1)}, f32[256,1]{0,1:T(1,128)}, u32[]{:S(2)}) copy-start(f32[256,1]{0,1:T(1,128)} %param.34) | copy-start | bytes 3076
  6.5 23.4 %copy-start.8 = (bf16[2048,128]{1,0:T(8,128)(2,1)S(1)}, bf16[2048,128]{1,0:T(8,128)(2,1)}, u32[]{:S(2)}) copy-start(bf16[2048,128]{1,0:T(8,128)(2,1)} %wr_ref.1) | copy-start | bytes 1572868
  6.5 23.4 %copy-start.9 = (bf16[2048,128]{1,0:T(8,128)(2,1)S(1)}, bf16[2048,128]{1,0:T(8,128)(2,1)}, u32[]{:S(2)}) copy-start(bf16[2048,128]{1,0:T(8,128)(2,1)} %wk_ref.2) | copy-start | bytes 1572868
  6.6 23.4 %copy-start.10 = (bf16[2048,128]{1,0:T(8,128)(2,1)S(1)}, bf16[2048,128]{1,0:T(8,128)(2,1)}, u32[]{:S(2)}) copy-start(bf16[2048,128]{1,0:T(8,128)(2,1)} %wv_ref.2) | copy-start | bytes 1572868
  6.6 23.4 %copy-start.15 = (bf16[64,128]{1,0:T(8,128)(2,1)S(1)}, bf16[64,128]{1,0:T(8,128)(2,1)}, u32[]{:S(2)}) copy-start(bf16[64,128]{1,0:T(8,128)(2,1)} %up_ref.1) | copy-start | bytes 49156
  6.6 92.9 %all-gather.3.cloned.1.call-start = ((), (), s32[]{:S(2)}) async-start(), calls=%async_computation.4 | async-start | bytes 2228224 | tf_op jit(solution)/shard_map/all_gather | solution.py:484
  21.3 3.8 %collective-permute-start = (bf16[4,256,256]{2,1,0:T(8,128)(2,1)S(1)}, bf16[4,256,256]{2,1,0:T(8,128)(2,1)S(1)}, u32[]{:S(2)}, u32[]{:S(2)}) collective-permute-start(bf16[4,256,256]{2,1,0:T(8,128)(2,1)S(1)} %all_to_all.20.own_ref), channel_id=1, source_target_pairs={{0,1},{1,0},{2,3},{3,2},{4,5},{5,4},{6,7},{7,6},{8,9},{9,8},{10,11... | collective-permute-start | bytes 1572872 | tf_op jit(solution)/shard_map/ppermute | solution.py:418
  25.0 1.0 copy-start
  26.1 1.0 copy-start.1
  27.1 0.7 copy-start.4
  27.8 2.2 %copy-start.11 = (bf16[2048,128]{1,0:T(8,128)(2,1)S(1)}, bf16[2048,128]{1,0:T(8,128)(2,1)}, u32[]{:S(2)}) copy-start(bf16[2048,128]{1,0:T(8,128)(2,1)} %wq_ref.1) | copy-start | bytes 1572868
  27.8 2.2 %copy-start.12 = (bf16[2048,64]{0,1:T(8,128)(2,1)S(1)}, bf16[2048,64]{0,1:T(8,128)(2,1)}, u32[]{:S(2)}) copy-start(bf16[2048,64]{0,1:T(8,128)(2,1)} %param.24) | copy-start | bytes 786436
  30.0 0.9 copy-start.13
  39.3 48.4 %copy-start.14 = (f32[2,64,64]{2,1,0:T(8,128)S(1)}, f32[2,64,64]{2,1,0:T(8,128)}, u32[]{:S(2)}) copy-start(f32[2,64,64]{2,1,0:T(8,128)} %state_ref.1) | copy-start | bytes 98308
  39.3 48.4 %copy-start.19 = (f32[128]{0:T(128)S(1)}, f32[128]{0:T(128)}, u32[]{:S(2)}) copy-start(f32[128]{0:T(128)} %param.29) | copy-start | bytes 1540
  91.3 44.3 %copy-start.2 = (bf16[128,2048]{1,0:T(8,128)(2,1)S(1)}, bf16[128,2048]{1,0:T(8,128)(2,1)}, u32[]{:S(2)}) copy-start(bf16[128,2048]{1,0:T(8,128)(2,1)} %wl_ref.1) | copy-start | bytes 1572868
  91.3 44.3 %copy-start.3 = (bf16[128,2048]{1,0:T(8,128)(2,1)S(1)}, bf16[128,2048]{1,0:T(8,128)(2,1)}, u32[]{:S(2)}) copy-start(bf16[128,2048]{1,0:T(8,128)(2,1)} %wa_ref.1) | copy-start | bytes 1572868
  91.3 44.3 %copy-start.6 = (f32[128]{0:T(128)S(1)}, f32[128]{0:T(128)}, u32[]{:S(2)}) copy-start(f32[128]{0:T(128)} %param.35) | copy-start | bytes 1540
  99.5 1.6 copy-start.7
  137.0 3.8 %collective-permute-start.1 = (bf16[4,256,256]{2,1,0:T(8,128)(2,1)S(1)}, bf16[4,256,256]{2,1,0:T(8,128)(2,1)S(1)}, u32[]{:S(2)}, u32[]{:S(2)}) collective-permute-start(bf16[4,256,256]{2,1,0:T(8,128)(2,1)S(1)} %get-tuple-element.24), channel_id=1, source_target_pairs={{0,1},{1,0},{2,3},{3,2},{4,5},{5,4},{6,7},{7,6},{8,9},{9,8},{10,11... | collective-permute-start | bytes 1572872 | tf_op jit(solution)/shard_map/ppermute | solution.py:418
Sparse Core Ops, SparseCore 0:
  30.0 69.4 all-gather.2

commit v3 on v2

--- a/solution.py
+++ b/solution.py
@@ -82,6 +82,12 @@
 
 def stacked(a):
     return jnp.concatenate([a[:, :WIDE], a[:, WIDE:]], axis=0)
+
+
+def spread_kernel(place_ref, tokens_ref, out_ref):
+    tokens = tokens_ref[...]
+    for j in range(out_ref.shape[0]):
+        out_ref[j] = tokens
 
 
 def kv_kernel(place_ref, own_ref, other_ref, gain_ref, wk_ref, wv_ref, out_ref):
@@ -327,28 +333,20 @@
 
 
 def att_kernel(
-    place_ref, asked_ref, held_ref, keys_ref, out_ref, best_ref, sum_ref, block_ref, sems, *, rows
+    place_ref, asked_ref, held_ref, keys_ref, out_ref, best_ref, sum_ref, *, rows
 ):
     z, y = place_ref[0], place_ref[1]
     count = asked_ref.shape[0]
     scale = HEAD_ATT ** (-0.5) * LOG2E
 
-    def fetch(k):
-        start = pl.multiple_of(k * 2 * rows, 2 * rows)
-        return pltpu.make_async_copy(
-            keys_ref.at[pl.ds(start, 2 * rows)], block_ref.at[k], sems.at[k]
-        )
-
-    lax.fori_loop(0, z + 1, lambda k, c: (fetch(k).start(), c)[1], 0)
     best_ref[...] = jnp.full(best_ref.shape, NEG, F32)
     sum_ref[...] = jnp.zeros(sum_ref.shape, F32)
     ones = jnp.ones((16, rows), BF16)
     base = joined(asked_ref[0, rows + WIDE : rows + WIDE + 16])[0:1, 0:1]
 
     def block(k, masked):
-        fetch(k).wait()
-        key = block_ref[k, 0:rows]
-        left, right = block_ref[k, rows : rows + WIDE], block_ref[k, rows + WIDE :]
+        both = keys_ref[k]
+        key, left, right = both[:rows], both[rows : rows + WIDE], both[rows + WIDE :]
         value = jnp.concatenate([jnp.concatenate([left, right], axis=1), ones], axis=0)
         drop = (base - joined(held_ref[k, WIDE : WIDE + 16])) * LOG2E
         drop = [jnp.broadcast_to(drop[i : i + 1], (WIDE, WIDE)).T for i in range(2)]
@@ -426,19 +424,14 @@
     return pl.BlockSpec(memory_space=pltpu.VMEM)
 
 
-def hbm():
-    return pl.BlockSpec(memory_space=pltpu.HBM)
-
-
-def call(kernel, name, shapes, flops, size, mib, scratch=(), outside=0):
+def call(kernel, name, shapes, flops, size, mib, scratch=()):
     def run(*operands):
         many = isinstance(shapes, (list, tuple))
-        inside = len(operands) - 1 - outside
         return pl.pallas_call(
             kernel,
             name=name,
             out_shape=shapes,
-            in_specs=[smem()] + [vmem()] * inside + [hbm()] * outside,
+            in_specs=[smem()] + [vmem()] * (len(operands) - 1),
             out_specs=[vmem()] * len(shapes) if many else vmem(),
             scratch_shapes=list(scratch),
             compiler_params=params(mib),
@@ -476,12 +469,15 @@
     place = jnp.stack([lax.axis_index(axis) for axis in ("z", "y", "c")]).astype(jnp.int32)
     gain = norm_gain.reshape(1, -1)
 
-    own = sent_to_all(tokens, "x")
+    copies = call(spread_kernel, "spread", shape((nx, *tokens.shape), BF16), 10**10, 1 << 24, 4)(
+        place, tokens
+    )
+    own = lax.all_to_all(copies, "x", 0, 0, tiled=True)
     other = to_other_core(own)
     kv = call(
         kv_kernel, "kv", shape((2 * rows, WIDE), BF16), 2 * rows * model_width * 256, 1 << 21, 12
     )(place, own, other, gain, att_key_weight, att_value_weight)
-    keys = lax.all_gather(kv, "z", axis=0, tiled=True)
+    keys = lax.all_gather(kv, "z")
 
     extra = 16
     send, gates, reach, local = call(
@@ -537,10 +533,7 @@
         scratch=[
             pltpu.VMEM((ny, 1, rows), F32),
             pltpu.VMEM((ny, HEAD_ATT + 16, rows), F32),
-            pltpu.VMEM((nz, 2 * rows, WIDE), BF16),
-            pltpu.SemaphoreType.DMA((nz,)),
         ],
-        outside=1,
     )(place, asked, held, keys)
     parts = lax.all_to_all(found, "y", 0, 0, tiled=True)
     width = model_width // (2 * nx)

time: 163 us -> 158 us (0.969)
  local copies, waits for them, and re-layouts: 6.45 us -> 3.54 us
  Pallas kernels: 40.5 us -> 38.1 us
    all_to_all x0 -> x1, blocking collectives: none -> 13.7 us  [body(): own = lax.all_to_all(copies, 'x', 0, 0, tiled=True)]
    all_to_all x2 -> x1, blocking collectives: 26.4 us -> 12.8 us  [sent_to_all(): lax.all_to_all(jnp.broadcast_to(a[None], (size, *a.shape)), axis, 0, 0, t...]
    pallas_call x6 -> x7, Pallas kernels: 40.5 us -> 38.1 us  [run(): pl.pallas_call(kernel, name=name, out_shape=shapes, in_specs=[smem()] + [...]
    unnamed x40, local copies, waits for them, and re-layouts: 5.34 us -> 3.49 us
where the time goes in v3:
time: 158 us
  blocking collectives  86.1 us (54%)
  Pallas kernels  38.1 us (24%)
  between operations  13.6 us (9%)
  waiting for transfers between devices  11.5 us (7%)
  starting transfers between devices  3.83 us (2%)
  local copies, waits for them, and re-layouts  3.54 us (2%)
    pallas_call x7, Pallas kernels, run(): pl.pallas_call(kernel, name=name, out_shape=shapes, in_specs=[smem()] + [...  38.1 us
    all_gather x1, blocking collectives, body(): held = lax.all_gather(row_send, 'z')  34.7 us
    all_to_all x1, blocking collectives, body(): tiles = lax.all_to_all(pair, 'x', 0, 0, tiled=True)  13.9 us
    all_to_all x1, blocking collectives, body(): own = lax.all_to_all(copies, 'x', 0, 0, tiled=True)  13.7 us
    all_to_all x1, blocking collectives, sent_to_all(): lax.all_to_all(jnp.broadcast_to(a[None], (size, *a.shape)), axis, 0, 0, t...  12.8 us
    all_to_all x1, blocking collectives, body(): parts = lax.all_to_all(found, 'y', 0, 0, tiled=True)  11 us
    all_gather x1, waiting for transfers between devices, body(): keys = lax.all_gather(kv, 'z')  7.74 us
    ppermute x2, starting transfers between devices, to_other_core(): return lax.ppermute(a, 'c', [(0, 1), (1, 0)])  3.83 us
  transfers between devices with their start and end apart: 3, of which 3 were waited for; matrix products, arithmetic and copies ran while one was open for 0% of the time, Pallas kernels for 8%

profile of v3, /device:TPU:480, one launch (start us, length us, event | category | flops | bytes accessed | tf_op | source)
XLA Modules:
  0.0 157.7 jit_solution(16132348279392408131)
XLA Ops:
  6.5 0.1 pad_add_fusion.place_ref
  6.6 0.9 copy-done.12
  7.5 0.6 spread.1
  8.1 0.0 copy-start.7
  8.1 0.0 copy-start.8
  8.1 0.0 copy-start.9
  8.1 0.0 copy-start.10
  8.2 0.0 copy-start.11
  8.2 0.0 copy-start.15
  8.2 0.0 copy-start.16
  8.2 0.0 copy-start.17
  8.2 0.0 copy-start.18
  8.2 13.7 %all_to_all.20.own_ref = bf16[4,256,256]{2,1,0:T(8,128)(2,1)S(1)} all-to-all(bf16[4,256,256]{2,1,0:T(8,128)(2,1)S(1)} %spread.1), channel_id=1, replica_groups=mesh['z'=16,'y'=4,'x'=4,'c'=2] {'x'}, dimensions={0} | all-to-all | bytes 1048576 | tf_op jit(solution)/shard_map/all_to_all | solution.py:475
  21.9 1.9 %collective-permute-start = (bf16[4,256,256]{2,1,0:T(8,128)(2,1)S(1)}, bf16[4,256,256]{2,1,0:T(8,128)(2,1)S(1)}, u32[]{:S(2)}, u32[]{:S(2)}) collective-permute-start(bf16[4,256,256]{2,1,0:T(8,128)(2,1)S(1)} %all_to_all.20.own_ref), channel_id=1, source_target_pairs={{0,1},{1,0},{2,3},{3,2},{4,5},{5,4},{6,7},{7,6},{8,9},{9,8},{10,11... | collective-permute-start | bytes 1572872 | tf_op jit(solution)/shard_map/ppermute | solution.py:416
  23.8 1.9 %collective-permute-done.other_ref = bf16[4,256,256]{2,1,0:T(8,128)(2,1)S(1)} collective-permute-done((bf16[4,256,256]{2,1,0:T(8,128)(2,1)S(1)}, bf16[4,256,256]{2,1,0:T(8,128)(2,1)S(1)}, u32[]{:S(2)}, u32[]{:S(2)}) %collective-permute-start) | collective-permute-done | bytes 524320 | tf_op jit(solution)/shard_map/ppermute | solution.py:416
  25.7 2.0 %kv.1 = bf16[512,128]{1,0:T(8,128)(2,1)} custom-call(s32[3]{0:T(128)S(1)} %pad_add_fusion.place_ref, bf16[4,256,256]{2,1,0:T(8,128)(2,1)S(1)} %all_to_all.20.own_ref, bf16[4,256,256]{2,1,0:T(8,128)(2,1)S(1)} %collective-permute-done.other_ref, f32[1,2048]{1,0:T(1,128)S(1)} %bitcast.14, bf16[2048,128]{1,0:T(8,128)(2,1)S(1)} %copy-done, ...), custom_call_target="tpu_custom_call" | custom-call | flops 268435456 | bytes 2097152 | tf_op jit(solution)/shard_map/kv/pallas_call | solution.py:430
  27.8 0.0 all-gather.4.cloned.1.call-update
  27.8 0.0 copy-done.7
  27.8 0.0 copy-done.8
  27.8 0.0 copy-done.9
  27.8 0.0 copy-done.10
  27.8 0.0 copy-done.11
  27.8 0.0 copy-done.15
  27.9 0.0 copy-done.16
  27.9 0.0 copy-done.17
  27.9 0.0 copy-done.18
  27.9 0.0 copy-start.13
  27.9 0.9 copy-done.13
  28.8 8.4 %lin.1 = (bf16[400,128]{1,0:T(8,128)(2,1)S(1)}, bf16[16,128]{1,0:T(8,128)(2,1)S(1)}, f32[256,128]{1,0:T(8,128)S(1)}, f32[256,128]{1,0:T(8,128)S(1)}) custom-call(s32[3]{0:T(128)S(1)} %pad_add_fusion.place_ref, bf16[4,256,256]{2,1,0:T(8,128)(2,1)S(1)} %all_to_all.20.own_ref, bf16[4,256,256]{2,1,0:T(8,128)(2,1)S(1)} %collective-permute-done.other_ref, ...), custom_call_target="tpu_custom_call" | custom-call | flops 4000000000 | bytes 4194304 | tf_op jit(solution)/shard_map/lin/pallas_call | solution.py:430
  37.2 0.0 copy-start.14
  37.2 0.0 copy-start.19
  37.2 0.1 broadcast_in_dim.2
  37.3 12.8 %all_to_all.21.gathered_ref.asked_ref = bf16[4,400,128]{2,1,0:T(8,128)(2,1)S(1)} all-to-all(bf16[4,400,128]{2,1,0:T(8,128)(2,1)S(1)} %broadcast_in_dim.2), channel_id=1, replica_groups=mesh['z'=16,'y'=4,'x'=4,'c'=2] {'y'}, dimensions={0} | all-to-all | bytes 819200 | tf_op jit(solution)/shard_map/all_to_all | solution.py:412
  50.1 1.1 row.1
  51.2 34.7 %all-gather = bf16[2304,128]{1,0:T(8,128)(2,1)S(1)} all-gather(bf16[144,128]{1,0:T(8,128)(2,1)S(1)} %get-tuple-element.17), channel_id=2, replica_groups=mesh['z'=16,'y'=4,'x'=4,'c'=2] {'z'}, dimensions={0}, use_global_device_ids=true | all-gather | bytes 626688 | tf_op jit(solution)/shard_map/all_gather | solution.py:521
  85.9 3.6 %mix.1.lin_ref = bf16[256,128]{1,0:T(8,128)(2,1)S(1)} custom-call(s32[3]{0:T(128)S(1)} %pad_add_fusion.place_ref, f32[2,64,64]{2,1,0:T(8,128)S(1)} %copy-done.14, bf16[16,144,128]{2,1,0:T(8,128)(2,1)S(1)} %bitcast.12, f32[2,128,128]{2,1,0:T(8,128)S(1)} %get-tuple-element.18.before_ref, f32[256,128]{1,0:T(8,128)S(1)} %get-tuple-element.19.reach_ref, ...), custom_call_target="tpu_custom_call" | custom-call | flops 1000000000 | bytes 1048576 | tf_op jit(solution)/shard_map/mix/pallas_call | solution.py:430
  89.5 7.7 %all-gather.4.cloned.1.call-done = bf16[8192,128]{1,0:T(8,128)(2,1)} async-done(((bf16[512,128]{1,0:T(8,128)(2,1)}), bf16[8192,128]{1,0:T(8,128)(2,1)}) %all-gather.4.cloned.1.call-update) | async-done | bytes 2097168 | tf_op jit(solution)/shard_map/all_gather | solution.py:480
  97.3 1.6 %copy-done.6 = bf16[8192,128]{1,0:T(8,128)(2,1)S(1)} copy-done((bf16[8192,128]{1,0:T(8,128)(2,1)S(1)}, bf16[8192,128]{1,0:T(8,128)(2,1)}, u32[]{:S(2)}) %copy-start.6) | copy-done | bytes 2097176
  98.9 21.0 %att.1 = bf16[4,144,256]{2,1,0:T(8,128)(2,1)S(1)} custom-call(s32[3]{0:T(128)S(1)} %pad_add_fusion.place_ref, bf16[4,400,128]{2,1,0:T(8,128)(2,1)S(1)} %all_to_all.21.gathered_ref.asked_ref, bf16[16,144,128]{2,1,0:T(8,128)(2,1)S(1)} %bitcast.13, bf16[16,512,128]{2,1,0:T(8,128)(2,1)S(1)} %bitcast.17), custom_call_target="tpu_custom_call" | custom-call | flops 2147483648 | bytes 4194304 | tf_op jit(solution)/shard_map/att/pallas_call | solution.py:430
  119.9 11.0 %all_to_all.22.parts_ref = bf16[4,144,256]{2,1,0:T(8,128)(2,1)S(1)} all-to-all(bf16[4,144,256]{2,1,0:T(8,128)(2,1)S(1)} %att.1), channel_id=1, replica_groups=mesh['z'=16,'y'=4,'x'=4,'c'=2] {'y'}, dimensions={0} | all-to-all | bytes 589824 | tf_op jit(solution)/shard_map/all_to_all | solution.py:538
  130.8 0.0 copy-done.2
  130.8 0.0 copy-done.5
  130.8 1.4 out.1
  132.2 1.9 %collective-permute-start.1 = (bf16[4,256,256]{2,1,0:T(8,128)(2,1)S(1)}, bf16[4,256,256]{2,1,0:T(8,128)(2,1)S(1)}, u32[]{:S(2)}, u32[]{:S(2)}) collective-permute-start(bf16[4,256,256]{2,1,0:T(8,128)(2,1)S(1)} %get-tuple-element.24), channel_id=1, source_target_pairs={{0,1},{1,0},{2,3},{3,2},{4,5},{5,4},{6,7},{7,6},{8,9},{9,8},{10,11... | collective-permute-start | bytes 1572872 | tf_op jit(solution)/shard_map/ppermute | solution.py:416
  134.2 1.9 %collective-permute-done.1 = bf16[4,256,256]{2,1,0:T(8,128)(2,1)S(1)} collective-permute-done((bf16[4,256,256]{2,1,0:T(8,128)(2,1)S(1)}, bf16[4,256,256]{2,1,0:T(8,128)(2,1)S(1)}, u32[]{:S(2)}, u32[]{:S(2)}) %collective-permute-start.1) | collective-permute-done | bytes 524320 | tf_op jit(solution)/shard_map/ppermute | solution.py:416
  136.0 0.1 add_convert_fusion
  136.2 13.9 %all_to_all.23 = bf16[4,256,256]{2,1,0:T(8,128)(2,1)S(1)} all-to-all(bf16[4,256,256]{2,1,0:T(8,128)(2,1)S(1)} %add_convert_fusion), channel_id=1, replica_groups=mesh['z'=16,'y'=4,'x'=4,'c'=2] {'x'}, dimensions={0} | all-to-all | bytes 1048576 | tf_op jit(solution)/shard_map/all_to_all | solution.py:545
  150.1 0.7 reduce_sum.12
  (15 shorter events, 0.0 us)
Async XLA Ops:
  6.5 90.7 %all-gather.4.cloned.1.call-start = ((), (), s32[]{:S(2)}) async-start(), calls=%async_computation.4 | async-start | bytes 2228224 | tf_op jit(solution)/shard_map/all_gather | solution.py:480
  6.6 0.9 copy-start.12
  7.5 18.2 %copy-start = (bf16[2048,128]{1,0:T(8,128)(2,1)S(1)}, bf16[2048,128]{1,0:T(8,128)(2,1)}, u32[]{:S(2)}) copy-start(bf16[2048,128]{1,0:T(8,128)(2,1)} %wk_ref.3) | copy-start | bytes 1572868
  7.5 18.2 %copy-start.1 = (bf16[2048,128]{1,0:T(8,128)(2,1)S(1)}, bf16[2048,128]{1,0:T(8,128)(2,1)}, u32[]{:S(2)}) copy-start(bf16[2048,128]{1,0:T(8,128)(2,1)} %wv_ref.3) | copy-start | bytes 1572868
  7.5 18.2 %copy-start.4 = (f32[2048]{0:T(1024)S(1)}, f32[2048]{0:T(1024)}, u32[]{:S(2)}) copy-start(f32[2048]{0:T(1024)} %param.20) | copy-start | bytes 24580
  8.1 19.7 %copy-start.7 = (bf16[2048,128]{1,0:T(8,128)(2,1)S(1)}, bf16[2048,128]{1,0:T(8,128)(2,1)}, u32[]{:S(2)}) copy-start(bf16[2048,128]{1,0:T(8,128)(2,1)} %wr_ref.1) | copy-start | bytes 1572868
  8.1 19.7 %copy-start.8 = (bf16[2048,128]{1,0:T(8,128)(2,1)S(1)}, bf16[2048,128]{1,0:T(8,128)(2,1)}, u32[]{:S(2)}) copy-start(bf16[2048,128]{1,0:T(8,128)(2,1)} %wk_ref.2) | copy-start | bytes 1572868
  8.1 19.7 %copy-start.9 = (bf16[2048,128]{1,0:T(8,128)(2,1)S(1)}, bf16[2048,128]{1,0:T(8,128)(2,1)}, u32[]{:S(2)}) copy-start(bf16[2048,128]{1,0:T(8,128)(2,1)} %wv_ref.2) | copy-start | bytes 1572868
  8.1 19.7 %copy-start.10 = (bf16[2048,128]{1,0:T(8,128)(2,1)S(1)}, bf16[2048,128]{1,0:T(8,128)(2,1)}, u32[]{:S(2)}) copy-start(bf16[2048,128]{1,0:T(8,128)(2,1)} %wq_ref.1) | copy-start | bytes 1572868
  8.2 19.7 %copy-start.11 = (bf16[2048,64]{0,1:T(8,128)(2,1)S(1)}, bf16[2048,64]{0,1:T(8,128)(2,1)}, u32[]{:S(2)}) copy-start(bf16[2048,64]{0,1:T(8,128)(2,1)} %param.24) | copy-start | bytes 786436
  8.2 19.7 %copy-start.15 = (bf16[64,128]{1,0:T(8,128)(2,1)S(1)}, bf16[64,128]{1,0:T(8,128)(2,1)}, u32[]{:S(2)}) copy-start(bf16[64,128]{1,0:T(8,128)(2,1)} %up_ref.1) | copy-start | bytes 49156
  8.2 19.7 %copy-start.16 = (f32[256,1]{0,1:T(1,128)S(1)}, f32[256,1]{0,1:T(1,128)}, u32[]{:S(2)}) copy-start(f32[256,1]{0,1:T(1,128)} %param.34) | copy-start | bytes 3076
  8.2 19.7 %copy-start.17 = (f32[128]{0:T(128)S(1)}, f32[128]{0:T(128)}, u32[]{:S(2)}) copy-start(f32[128]{0:T(128)} %param.26) | copy-start | bytes 1540
  8.2 19.7 %copy-start.18 = (f32[128]{0:T(128)S(1)}, f32[128]{0:T(128)}, u32[]{:S(2)}) copy-start(f32[128]{0:T(128)} %param.28) | copy-start | bytes 1540
  21.9 3.8 %collective-permute-start = (bf16[4,256,256]{2,1,0:T(8,128)(2,1)S(1)}, bf16[4,256,256]{2,1,0:T(8,128)(2,1)S(1)}, u32[]{:S(2)}, u32[]{:S(2)}) collective-permute-start(bf16[4,256,256]{2,1,0:T(8,128)(2,1)S(1)} %all_to_all.20.own_ref), channel_id=1, source_target_pairs={{0,1},{1,0},{2,3},{3,2},{4,5},{5,4},{6,7},{7,6},{8,9},{9,8},{10,11... | collective-permute-start | bytes 1572872 | tf_op jit(solution)/shard_map/ppermute | solution.py:416
  27.9 0.9 copy-start.13
  37.2 48.7 %copy-start.14 = (f32[2,64,64]{2,1,0:T(8,128)S(1)}, f32[2,64,64]{2,1,0:T(8,128)}, u32[]{:S(2)}) copy-start(f32[2,64,64]{2,1,0:T(8,128)} %state_ref.1) | copy-start | bytes 98308
  37.2 48.7 %copy-start.19 = (f32[128]{0:T(128)S(1)}, f32[128]{0:T(128)}, u32[]{:S(2)}) copy-start(f32[128]{0:T(128)} %param.29) | copy-start | bytes 1540
  97.3 1.6 %copy-start.6 = (bf16[8192,128]{1,0:T(8,128)(2,1)S(1)}, bf16[8192,128]{1,0:T(8,128)(2,1)}, u32[]{:S(2)}) copy-start(bf16[8192,128]{1,0:T(8,128)(2,1)} %all-gather.4.cloned.1.call-done) | copy-start | bytes 6291460
  98.9 32.0 %copy-start.2 = (bf16[128,2048]{1,0:T(8,128)(2,1)S(1)}, bf16[128,2048]{1,0:T(8,128)(2,1)}, u32[]{:S(2)}) copy-start(bf16[128,2048]{1,0:T(8,128)(2,1)} %wl_ref.1) | copy-start | bytes 1572868
  98.9 32.0 %copy-start.3 = (bf16[128,2048]{1,0:T(8,128)(2,1)S(1)}, bf16[128,2048]{1,0:T(8,128)(2,1)}, u32[]{:S(2)}) copy-start(bf16[128,2048]{1,0:T(8,128)(2,1)} %wa_ref.1) | copy-start | bytes 1572868
  98.9 32.0 %copy-start.5 = (f32[128]{0:T(128)S(1)}, f32[128]{0:T(128)}, u32[]{:S(2)}) copy-start(f32[128]{0:T(128)} %param.35) | copy-start | bytes 1540
  132.2 3.8 %collective-permute-start.1 = (bf16[4,256,256]{2,1,0:T(8,128)(2,1)S(1)}, bf16[4,256,256]{2,1,0:T(8,128)(2,1)S(1)}, u32[]{:S(2)}, u32[]{:S(2)}) collective-permute-start(bf16[4,256,256]{2,1,0:T(8,128)(2,1)S(1)} %get-tuple-element.24), channel_id=1, source_target_pairs={{0,1},{1,0},{2,3},{3,2},{4,5},{5,4},{6,7},{7,6},{8,9},{9,8},{10,11... | collective-permute-start | bytes 1572872 | tf_op jit(solution)/shard_map/ppermute | solution.py:416
Sparse Core Ops, SparseCore 0:
  27.9 69.3 all-gather.3

commit v4 on v3

--- a/solution.py
+++ b/solution.py
@@ -73,15 +73,12 @@
     return scaled, lax.rsqrt(mean + 1e-6)
 
 
-def projected(scaled, inverse, w_ref):
+def projected(scaled, inverse, *w_refs):
     total = 0.0
     for piece, start in scaled:
-        total = total + dot(piece, w_ref[pl.ds(start, piece.shape[1])])
+        weight = [w_ref[pl.ds(start, piece.shape[1])] for w_ref in w_refs]
+        total = total + dot(piece, jnp.concatenate(weight, axis=1))
     return total * inverse
-
-
-def stacked(a):
-    return jnp.concatenate([a[:, :WIDE], a[:, WIDE:]], axis=0)
 
 
 def spread_kernel(place_ref, tokens_ref, out_ref):
@@ -93,8 +90,9 @@
 def kv_kernel(place_ref, own_ref, other_ref, gain_ref, wk_ref, wv_ref, out_ref):
     scaled, inverse = scaled_pieces(place_ref, own_ref, other_ref, gain_ref)
     rows = own_ref.shape[1]
-    out_ref[0:rows] = projected(scaled, inverse, wk_ref).astype(BF16)
-    out_ref[rows:] = stacked(projected(scaled, inverse, wv_ref).T.astype(BF16))
+    both = projected(scaled, inverse, wk_ref, wv_ref).astype(BF16)
+    out_ref[0:rows] = both[:, :HEAD_ATT]
+    out_ref[rows:] = both[:, HEAD_ATT:]
 
 
 def spans(log_decay):
@@ -148,10 +146,11 @@
 ):
     scaled, inverse = scaled_pieces(place_ref, own_ref, other_ref, gain_ref)
     rows = shift_ref.shape[0]
-    send_ref[0:rows] = stacked(projected(scaled, inverse, wq_ref).T.astype(BF16))
-    recv = projected(scaled, inverse, wr_ref).astype(BF16).astype(F32)
-    key = projected(scaled, inverse, wk_ref).astype(BF16).astype(F32)
-    value = projected(scaled, inverse, wv_ref).astype(BF16)
+    both = projected(scaled, inverse, wr_ref, wk_ref).astype(BF16)
+    recv, key = both[:, :WIDE].astype(F32), both[:, WIDE:].astype(F32)
+    both = projected(scaled, inverse, wv_ref, wq_ref).astype(BF16)
+    value = both[:, :WIDE]
+    send_ref[0:rows] = both[:, WIDE:]
     low = 0.0
     for piece, start in scaled:
         low = low + dot(piece, down_ref[:, pl.ds(start, piece.shape[1])], ((1,), (1,)))
@@ -333,71 +332,98 @@
 
 
 def att_kernel(
-    place_ref, asked_ref, held_ref, keys_ref, out_ref, best_ref, sum_ref, *, rows
+    place_ref, asked_ref, held_ref, keys_ref, out_ref, logit_ref, best_ref, sum_ref, *, rows
 ):
     z, y = place_ref[0], place_ref[1]
     count = asked_ref.shape[0]
     scale = HEAD_ATT ** (-0.5) * LOG2E
-
     best_ref[...] = jnp.full(best_ref.shape, NEG, F32)
     sum_ref[...] = jnp.zeros(sum_ref.shape, F32)
-    ones = jnp.ones((16, rows), BF16)
+    ones = jnp.ones((rows, HEAD_ATT), BF16)
     base = joined(asked_ref[0, rows + WIDE : rows + WIDE + 16])[0:1, 0:1]
 
-    def block(k, masked):
-        both = keys_ref[k]
-        key, left, right = both[:rows], both[rows : rows + WIDE], both[rows + WIDE :]
-        value = jnp.concatenate([jnp.concatenate([left, right], axis=1), ones], axis=0)
+    def score(k, masked):
+        key = keys_ref[k, 0:rows]
         drop = (base - joined(held_ref[k, WIDE : WIDE + 16])) * LOG2E
-        drop = [jnp.broadcast_to(drop[i : i + 1], (WIDE, WIDE)).T for i in range(2)]
-        drop = jnp.concatenate(drop, axis=0)
-        drop = jnp.concatenate([drop, drop], axis=1)
+        drop = jnp.concatenate([drop[0:1], drop[1:2]], axis=1)
         for j in range(count):
-            asked = jnp.concatenate([asked_ref[j, 0:WIDE], asked_ref[j, WIDE:rows]], axis=1)
-            logits = dot(key, asked) * scale + drop
+            logits = dot(asked_ref[j, 0:rows], key, ((1,), (1,))) * scale + drop
             if masked:
-                allowed = y * rows + iota(logits.shape, 0) <= j * rows + iota(logits.shape, 1)
+                allowed = y * rows + iota(logits.shape, 1) <= j * rows + iota(logits.shape, 0)
                 logits = jnp.where(allowed, logits, NEG)
-            old = best_ref[j]
-            new = jnp.maximum(old, jnp.max(logits, axis=0, keepdims=True))
-            weights = jnp.exp2(logits - new)
-            if masked:
-                weights = jnp.where(allowed, weights, 0.0)
-            sum_ref[j] = sum_ref[j] * jnp.exp2(old - new) + dot(value, weights.astype(BF16))
-            best_ref[j] = new
-
-    lax.fori_loop(0, z, lambda k, c: (block(k, False), c)[1], 0)
-    block(z, True)
-    third = iota((16, rows), 0)
+            logit_ref[k, j] = logits
+            top = functools.reduce(
+                jnp.maximum, [logits[:, i : i + WIDE] for i in range(0, rows, WIDE)]
+            )
+            best_ref[j] = jnp.maximum(best_ref[j], top)
+
+    def gather(*blocks):
+        value = [jnp.concatenate([keys_ref[k, rows:], ones], axis=1) for k in blocks]
+        for j in range(count):
+            best = jnp.concatenate([best_ref[j]] * (rows // WIDE), axis=1)
+            new = 0.0
+            for k, v in zip(blocks, value):
+                new = new + dot(jnp.exp2(logit_ref[k, j] - best).astype(BF16), v)
+            sum_ref[j] = sum_ref[j] + new
+
+    def score_many(i, carry):
+        for k in range(5):
+            score(5 * i + k, False)
+        return carry
+
+    def score_one(k, carry):
+        score(k, False)
+        return carry
+
+    def gather_many(i, carry):
+        gather(*(8 * i + k for k in range(8)))
+        return carry
+
+    def gather_one(k, carry):
+        gather(k)
+        return carry
+
+    many = z // 5
+    lax.fori_loop(0, many, score_many, 0)
+    lax.fori_loop(5 * many, z, score_one, 0)
+    score(z, True)
     for j in range(count):
-        total = sum_ref[j, HEAD_ATT : HEAD_ATT + 1]
+        best = jnp.max(best_ref[j], axis=1, keepdims=True)
+        best = jnp.where(best > 0.5 * NEG, best, 0.0)
+        best_ref[j] = jnp.broadcast_to(best, best_ref.shape[1:])
+    many = (z + 1) // 8
+    lax.fori_loop(0, many, gather_many, 0)
+    lax.fori_loop(8 * many, z + 1, gather_one, 0)
+    third = iota((rows, WIDE), 1)
+    for j in range(count):
+        total = sum_ref[j, :, HEAD_ATT:]
         some = total > 0.0
         safe = jnp.where(some, total, 1.0)
-        out_ref[j, 0:HEAD_ATT] = (sum_ref[j, 0:HEAD_ATT] / safe).astype(BF16)
+        out_ref[j, :, 0:HEAD_ATT] = (sum_ref[j, :, 0:HEAD_ATT] / safe).astype(BF16)
         level = jnp.where(some, best_ref[j] + jnp.log(safe) * LOG2E, NEG)
         high, mid = parts_of(level)
         high, mid = high.astype(F32), mid.astype(F32)
         last = level - high - mid
-        level = jnp.where(third == 0, high, jnp.where(third == 1, mid, last))
-        out_ref[j, HEAD_ATT:] = level.astype(BF16)
+        level = jnp.where(third < 40, high, jnp.where(third < 80, mid, last))
+        out_ref[j, :, HEAD_ATT:] = level.astype(BF16)
 
 
 def out_kernel(place_ref, parts_ref, lin_ref, gain_ref, wl_ref, wa_ref, own_ref, other_ref):
-    count, rows = parts_ref.shape[0], parts_ref.shape[2]
+    count, rows = parts_ref.shape[0], parts_ref.shape[1]
     core = place_ref[2]
     levels = []
     for j in range(count):
-        level = parts_ref[j, HEAD_ATT:].astype(F32)
-        levels.append(level[0:1] + level[1:2] + level[2:3])
+        level = parts_ref[j, :, HEAD_ATT:].astype(F32)
+        levels.append(level[:, 0:1] + level[:, 40:41] + level[:, 80:81])
     top = functools.reduce(jnp.maximum, levels)
-    total, raw = jnp.zeros((1, rows), F32), jnp.zeros((HEAD_ATT, rows), F32)
+    total, raw = jnp.zeros((rows, 1), F32), jnp.zeros((rows, HEAD_ATT), F32)
     for j in range(count):
         share = jnp.exp2(levels[j] - top)
         total = total + share
-        raw = raw + share * parts_ref[j, 0:HEAD_ATT].astype(F32)
+        raw = raw + share * parts_ref[j, :, 0:HEAD_ATT].astype(F32)
     raw = raw / total
-    size = jnp.mean(raw * raw, axis=0, keepdims=True)
-    att = ((raw * lax.rsqrt(size + 1e-6)).T * gain_ref[...]).astype(BF16)
+    size = jnp.mean(raw * raw, axis=1, keepdims=True)
+    att = (raw * lax.rsqrt(size + 1e-6) * gain_ref[...]).astype(BF16)
     lin = lin_ref[...]
     width = own_ref.shape[2]
     for c, ref in enumerate((own_ref, other_ref)):
@@ -526,13 +552,14 @@
     found = call(
         functools.partial(att_kernel, rows=rows),
         "att",
-        shape((ny, HEAD_ATT + 16, rows), BF16),
+        shape((ny, rows, HEAD_ATT + WIDE), BF16),
         ny * rows * nz * rows * 512,
         1 << 22,
-        24,
+        36,
         scratch=[
-            pltpu.VMEM((ny, 1, rows), F32),
-            pltpu.VMEM((ny, HEAD_ATT + 16, rows), F32),
+            pltpu.VMEM((nz, ny, rows, rows), F32),
+            pltpu.VMEM((ny, rows, WIDE), F32),
+            pltpu.VMEM((ny, rows, HEAD_ATT + WIDE), F32),
         ],
     )(place, asked, held, keys)
     parts = lax.all_to_all(found, "y", 0, 0, tiled=True)

time: 158 us -> 147 us (0.930); the launches traced: 158 us -> 145 us
  Pallas kernels: 38.1 us -> 23.1 us
  waiting for transfers between devices: 11.5 us -> 15.2 us
  blocking collectives: 86.1 us -> 84.4 us
    pallas_call x7, Pallas kernels: 38.1 us -> 23.1 us  [run(): pl.pallas_call(kernel, name=name, out_shape=shapes, in_specs=[smem()] + [...]
    all_gather x1, waiting for transfers between devices: 7.74 us -> 11.4 us  [body(): keys = lax.all_gather(kv, 'z')]
    all_gather x1, blocking collectives: 34.7 us -> 32.7 us  [body(): held = lax.all_gather(row_send, 'z')]
  transfers between devices with their start and end apart: 3 -> 3, of which waited for: 3 -> 3; matrix products, arithmetic and copies ran while one was open for 0% -> 0% of each run, Pallas kernels for 8% -> 9%
where the time goes in v4:
time: 147 us; the launch traced here: 145 us
  blocking collectives  84.4 us (57%)
  Pallas kernels  23.1 us (16%)
  waiting for transfers between devices  15.2 us (10%)
  between operations  13.6 us (9%)
  starting transfers between devices  3.83 us (3%)
  local copies, waits for them, and re-layouts  3.54 us (2%)
    all_gather x1, blocking collectives, body(): held = lax.all_gather(row_send, 'z')  32.7 us
    pallas_call x7, Pallas kernels, run(): pl.pallas_call(kernel, name=name, out_shape=shapes, in_specs=[smem()] + [...  23.1 us
    all_to_all x1, blocking collectives, body(): own = lax.all_to_all(copies, 'x', 0, 0, tiled=True)  13.7 us
    all_to_all x1, blocking collectives, body(): tiles = lax.all_to_all(pair, 'x', 0, 0, tiled=True)  13.3 us
    all_to_all x1, blocking collectives, sent_to_all(): lax.all_to_all(jnp.broadcast_to(a[None], (size, *a.shape)), axis, 0, 0, t...  12.8 us
    all_to_all x1, blocking collectives, body(): parts = lax.all_to_all(found, 'y', 0, 0, tiled=True)  12 us
    all_gather x1, waiting for transfers between devices, body(): keys = lax.all_gather(kv, 'z')  11.4 us
    ppermute x2, starting transfers between devices, to_other_core(): return lax.ppermute(a, 'c', [(0, 1), (1, 0)])  3.83 us
  transfers between devices with their start and end apart: 3, of which 3 were waited for; matrix products, arithmetic and copies ran while one was open for 0% of the time, Pallas kernels for 9%

profile of v4, /device:TPU:480, one launch (start us, length us, event | category | flops | bytes accessed | tf_op | source)
XLA Modules:
  0.0 144.7 jit_solution(11535458674761824340)
XLA Ops:
  6.5 0.1 pad_add_fusion.place_ref
  6.6 0.9 copy-done.12
  7.5 0.6 spread.1
  8.1 0.0 copy-start.7
  8.1 0.0 copy-start.8
  8.1 0.0 copy-start.9
  8.1 0.0 copy-start.10
  8.2 0.0 copy-start.11
  8.2 0.0 copy-start.15
  8.2 0.0 copy-start.16
  8.2 0.0 copy-start.17
  8.2 0.0 copy-start.18
  8.2 13.7 %all_to_all.20.own_ref = bf16[4,256,256]{2,1,0:T(8,128)(2,1)S(1)} all-to-all(bf16[4,256,256]{2,1,0:T(8,128)(2,1)S(1)} %spread.1), channel_id=1, replica_groups=mesh['z'=16,'y'=4,'x'=4,'c'=2] {'x'}, dimensions={0} | all-to-all | bytes 1048576 | tf_op jit(solution)/shard_map/all_to_all | solution.py:501
  21.9 1.9 %collective-permute-start = (bf16[4,256,256]{2,1,0:T(8,128)(2,1)S(1)}, bf16[4,256,256]{2,1,0:T(8,128)(2,1)S(1)}, u32[]{:S(2)}, u32[]{:S(2)}) collective-permute-start(bf16[4,256,256]{2,1,0:T(8,128)(2,1)S(1)} %all_to_all.20.own_ref), channel_id=1, source_target_pairs={{0,1},{1,0},{2,3},{3,2},{4,5},{5,4},{6,7},{7,6},{8,9},{9,8},{10,11... | collective-permute-start | bytes 1572872 | tf_op jit(solution)/shard_map/ppermute | solution.py:442
  23.8 1.9 %collective-permute-done.other_ref = bf16[4,256,256]{2,1,0:T(8,128)(2,1)S(1)} collective-permute-done((bf16[4,256,256]{2,1,0:T(8,128)(2,1)S(1)}, bf16[4,256,256]{2,1,0:T(8,128)(2,1)S(1)}, u32[]{:S(2)}, u32[]{:S(2)}) %collective-permute-start) | collective-permute-done | bytes 524320 | tf_op jit(solution)/shard_map/ppermute | solution.py:442
  25.7 0.0 copy-done
  25.7 0.0 copy-done.4
  25.7 1.7 %kv.1 = bf16[512,128]{1,0:T(8,128)(2,1)} custom-call(s32[3]{0:T(128)S(1)} %pad_add_fusion.place_ref, bf16[4,256,256]{2,1,0:T(8,128)(2,1)S(1)} %all_to_all.20.own_ref, bf16[4,256,256]{2,1,0:T(8,128)(2,1)S(1)} %collective-permute-done.other_ref, f32[1,2048]{1,0:T(1,128)S(1)} %bitcast.14, bf16[2048,128]{1,0:T(8,128)(2,1)S(1)} %copy-done, ...), custom_call_target="tpu_custom_call" | custom-call | flops 268435456 | bytes 2097152 | tf_op jit(solution)/shard_map/kv/pallas_call | solution.py:456
  27.4 0.0 all-gather.4.cloned.1.call-update
  27.4 0.0 copy-done.7
  27.5 0.0 copy-done.8
  27.5 0.0 copy-done.9
  27.5 0.0 copy-done.10
  27.5 0.0 copy-done.11
  27.5 0.0 copy-done.15
  27.5 0.0 copy-done.16
  27.5 0.0 copy-done.17
  27.5 0.0 copy-done.18
  27.5 0.0 copy-start.13
  27.6 0.9 copy-done.13
  28.4 7.8 %lin.1 = (bf16[400,128]{1,0:T(8,128)(2,1)S(1)}, bf16[16,128]{1,0:T(8,128)(2,1)S(1)}, f32[256,128]{1,0:T(8,128)S(1)}, f32[256,128]{1,0:T(8,128)S(1)}) custom-call(s32[3]{0:T(128)S(1)} %pad_add_fusion.place_ref, bf16[4,256,256]{2,1,0:T(8,128)(2,1)S(1)} %all_to_all.20.own_ref, bf16[4,256,256]{2,1,0:T(8,128)(2,1)S(1)} %collective-permute-done.other_ref, ...), custom_call_target="tpu_custom_call" | custom-call | flops 4000000000 | bytes 4194304 | tf_op jit(solution)/shard_map/lin/pallas_call | solution.py:456
  36.2 0.0 copy-start.19
  36.3 0.1 broadcast_in_dim.2
  36.3 12.8 %all_to_all.21.gathered_ref.asked_ref = bf16[4,400,128]{2,1,0:T(8,128)(2,1)S(1)} all-to-all(bf16[4,400,128]{2,1,0:T(8,128)(2,1)S(1)} %broadcast_in_dim.2), channel_id=1, replica_groups=mesh['z'=16,'y'=4,'x'=4,'c'=2] {'y'}, dimensions={0} | all-to-all | bytes 819200 | tf_op jit(solution)/shard_map/all_to_all | solution.py:438
  49.1 1.1 row.1
  50.2 32.7 %all-gather = bf16[2304,128]{1,0:T(8,128)(2,1)S(1)} all-gather(bf16[144,128]{1,0:T(8,128)(2,1)S(1)} %get-tuple-element.17), channel_id=2, replica_groups=mesh['z'=16,'y'=4,'x'=4,'c'=2] {'z'}, dimensions={0}, use_global_device_ids=true | all-gather | bytes 626688 | tf_op jit(solution)/shard_map/all_gather | solution.py:547
  82.9 3.6 %mix.1.lin_ref = bf16[256,128]{1,0:T(8,128)(2,1)S(1)} custom-call(s32[3]{0:T(128)S(1)} %pad_add_fusion.place_ref, f32[2,64,64]{2,1,0:T(8,128)S(1)} %copy-done.14, bf16[16,144,128]{2,1,0:T(8,128)(2,1)S(1)} %bitcast.12, f32[2,128,128]{2,1,0:T(8,128)S(1)} %get-tuple-element.18.before_ref, f32[256,128]{1,0:T(8,128)S(1)} %get-tuple-element.19.reach_ref, ...), custom_call_target="tpu_custom_call" | custom-call | flops 1000000000 | bytes 1048576 | tf_op jit(solution)/shard_map/mix/pallas_call | solution.py:456
  86.6 11.4 %all-gather.4.cloned.1.call-done = bf16[8192,128]{1,0:T(8,128)(2,1)} async-done(((bf16[512,128]{1,0:T(8,128)(2,1)}), bf16[8192,128]{1,0:T(8,128)(2,1)}) %all-gather.4.cloned.1.call-update) | async-done | bytes 2097168 | tf_op jit(solution)/shard_map/all_gather | solution.py:506
  98.0 1.6 %copy-done.6 = bf16[8192,128]{1,0:T(8,128)(2,1)S(1)} copy-done((bf16[8192,128]{1,0:T(8,128)(2,1)S(1)}, bf16[8192,128]{1,0:T(8,128)(2,1)}, u32[]{:S(2)}) %copy-start.6) | copy-done | bytes 2097176
  99.6 6.6 %att.1 = bf16[4,256,256]{2,1,0:T(8,128)(2,1)S(1)} custom-call(s32[3]{0:T(128)S(1)} %pad_add_fusion.place_ref, bf16[4,400,128]{2,1,0:T(8,128)(2,1)S(1)} %all_to_all.21.gathered_ref.asked_ref, bf16[16,144,128]{2,1,0:T(8,128)(2,1)S(1)} %bitcast.13, bf16[16,512,128]{2,1,0:T(8,128)(2,1)S(1)} %bitcast.17), custom_call_target="tpu_custom_call" | custom-call | flops 2147483648 | bytes 4194304 | tf_op jit(solution)/shard_map/att/pallas_call | solution.py:456
  106.2 12.0 %all_to_all.22.parts_ref = bf16[4,256,256]{2,1,0:T(8,128)(2,1)S(1)} all-to-all(bf16[4,256,256]{2,1,0:T(8,128)(2,1)S(1)} %att.1), channel_id=1, replica_groups=mesh['z'=16,'y'=4,'x'=4,'c'=2] {'y'}, dimensions={0} | all-to-all | bytes 1048576 | tf_op jit(solution)/shard_map/all_to_all | solution.py:565
  118.1 0.0 copy-done.5
  118.1 1.7 %out.1 = (bf16[4,256,256]{2,1,0:T(8,128)(2,1)S(1)}, bf16[4,256,256]{2,1,0:T(8,128)(2,1)S(1)}) custom-call(s32[3]{0:T(128)S(1)} %pad_add_fusion.place_ref, bf16[4,256,256]{2,1,0:T(8,128)(2,1)S(1)} %all_to_all.22.parts_ref, bf16[256,128]{1,0:T(8,128)(2,1)S(1)} %mix.1.lin_ref, f32[1,128]{1,0:T(1,128)S(1)} %bitcast.16, bf16[128,2048]{1,0:T(8,128)(2,1)S(1)} %copy-done.2, ...), custom_call_target="tpu_custom_call" | custom-call | flops 268435456 | bytes 2097152 | tf_op jit(solution)/shard_map/out/pallas_call | solution.py:456
  119.9 1.9 %collective-permute-start.1 = (bf16[4,256,256]{2,1,0:T(8,128)(2,1)S(1)}, bf16[4,256,256]{2,1,0:T(8,128)(2,1)S(1)}, u32[]{:S(2)}, u32[]{:S(2)}) collective-permute-start(bf16[4,256,256]{2,1,0:T(8,128)(2,1)S(1)} %get-tuple-element.24), channel_id=1, source_target_pairs={{0,1},{1,0},{2,3},{3,2},{4,5},{5,4},{6,7},{7,6},{8,9},{9,8},{10,11... | collective-permute-start | bytes 1572872 | tf_op jit(solution)/shard_map/ppermute | solution.py:442
  121.8 1.9 %collective-permute-done.1 = bf16[4,256,256]{2,1,0:T(8,128)(2,1)S(1)} collective-permute-done((bf16[4,256,256]{2,1,0:T(8,128)(2,1)S(1)}, bf16[4,256,256]{2,1,0:T(8,128)(2,1)S(1)}, u32[]{:S(2)}, u32[]{:S(2)}) %collective-permute-start.1) | collective-permute-done | bytes 524320 | tf_op jit(solution)/shard_map/ppermute | solution.py:442
  123.7 0.1 add_convert_fusion
  123.8 13.3 %all_to_all.23 = bf16[4,256,256]{2,1,0:T(8,128)(2,1)S(1)} all-to-all(bf16[4,256,256]{2,1,0:T(8,128)(2,1)S(1)} %add_convert_fusion), channel_id=1, replica_groups=mesh['z'=16,'y'=4,'x'=4,'c'=2] {'x'}, dimensions={0} | all-to-all | bytes 1048576 | tf_op jit(solution)/shard_map/all_to_all | solution.py:572
  137.1 0.7 reduce_sum.12
  (15 shorter events, 0.0 us)
Async XLA Ops:
  6.5 91.4 %all-gather.4.cloned.1.call-start = ((), (), s32[]{:S(2)}) async-start(), calls=%async_computation.4 | async-start | bytes 2228224 | tf_op jit(solution)/shard_map/all_gather | solution.py:506
  6.6 0.9 copy-start.12
  7.5 18.2 %copy-start = (bf16[2048,128]{1,0:T(8,128)(2,1)S(1)}, bf16[2048,128]{1,0:T(8,128)(2,1)}, u32[]{:S(2)}) copy-start(bf16[2048,128]{1,0:T(8,128)(2,1)} %wk_ref.3) | copy-start | bytes 1572868
  7.5 18.2 %copy-start.1 = (bf16[2048,128]{1,0:T(8,128)(2,1)S(1)}, bf16[2048,128]{1,0:T(8,128)(2,1)}, u32[]{:S(2)}) copy-start(bf16[2048,128]{1,0:T(8,128)(2,1)} %wv_ref.3) | copy-start | bytes 1572868
  7.5 18.2 %copy-start.4 = (f32[2048]{0:T(1024)S(1)}, f32[2048]{0:T(1024)}, u32[]{:S(2)}) copy-start(f32[2048]{0:T(1024)} %param.20) | copy-start | bytes 24580
  8.1 19.3 %copy-start.7 = (bf16[2048,128]{1,0:T(8,128)(2,1)S(1)}, bf16[2048,128]{1,0:T(8,128)(2,1)}, u32[]{:S(2)}) copy-start(bf16[2048,128]{1,0:T(8,128)(2,1)} %wr_ref.1) | copy-start | bytes 1572868
  8.1 19.3 %copy-start.8 = (bf16[2048,128]{1,0:T(8,128)(2,1)S(1)}, bf16[2048,128]{1,0:T(8,128)(2,1)}, u32[]{:S(2)}) copy-start(bf16[2048,128]{1,0:T(8,128)(2,1)} %wk_ref.2) | copy-start | bytes 1572868
  8.1 19.3 %copy-start.9 = (bf16[2048,128]{1,0:T(8,128)(2,1)S(1)}, bf16[2048,128]{1,0:T(8,128)(2,1)}, u32[]{:S(2)}) copy-start(bf16[2048,128]{1,0:T(8,128)(2,1)} %wv_ref.2) | copy-start | bytes 1572868
  8.1 19.3 %copy-start.10 = (bf16[2048,128]{1,0:T(8,128)(2,1)S(1)}, bf16[2048,128]{1,0:T(8,128)(2,1)}, u32[]{:S(2)}) copy-start(bf16[2048,128]{1,0:T(8,128)(2,1)} %wq_ref.1) | copy-start | bytes 1572868
  8.2 19.3 %copy-start.11 = (bf16[2048,64]{0,1:T(8,128)(2,1)S(1)}, bf16[2048,64]{0,1:T(8,128)(2,1)}, u32[]{:S(2)}) copy-start(bf16[2048,64]{0,1:T(8,128)(2,1)} %param.24) | copy-start | bytes 786436
  8.2 19.3 %copy-start.15 = (bf16[64,128]{1,0:T(8,128)(2,1)S(1)}, bf16[64,128]{1,0:T(8,128)(2,1)}, u32[]{:S(2)}) copy-start(bf16[64,128]{1,0:T(8,128)(2,1)} %up_ref.1) | copy-start | bytes 49156
  8.2 19.3 %copy-start.16 = (f32[256,1]{0,1:T(1,128)S(1)}, f32[256,1]{0,1:T(1,128)}, u32[]{:S(2)}) copy-start(f32[256,1]{0,1:T(1,128)} %param.34) | copy-start | bytes 3076
  8.2 19.3 %copy-start.17 = (f32[128]{0:T(128)S(1)}, f32[128]{0:T(128)}, u32[]{:S(2)}) copy-start(f32[128]{0:T(128)} %param.26) | copy-start | bytes 1540
  8.2 19.3 %copy-start.18 = (f32[128]{0:T(128)S(1)}, f32[128]{0:T(128)}, u32[]{:S(2)}) copy-start(f32[128]{0:T(128)} %param.28) | copy-start | bytes 1540
  21.9 3.8 %collective-permute-start = (bf16[4,256,256]{2,1,0:T(8,128)(2,1)S(1)}, bf16[4,256,256]{2,1,0:T(8,128)(2,1)S(1)}, u32[]{:S(2)}, u32[]{:S(2)}) collective-permute-start(bf16[4,256,256]{2,1,0:T(8,128)(2,1)S(1)} %all_to_all.20.own_ref), channel_id=1, source_target_pairs={{0,1},{1,0},{2,3},{3,2},{4,5},{5,4},{6,7},{7,6},{8,9},{9,8},{10,11... | collective-permute-start | bytes 1572872 | tf_op jit(solution)/shard_map/ppermute | solution.py:442
  27.5 0.9 copy-start.13
  36.2 46.7 %copy-start.14 = (f32[2,64,64]{2,1,0:T(8,128)S(1)}, f32[2,64,64]{2,1,0:T(8,128)}, u32[]{:S(2)}) copy-start(f32[2,64,64]{2,1,0:T(8,128)} %state_ref.1) | copy-start | bytes 98308
  36.2 46.7 %copy-start.19 = (f32[128]{0:T(128)S(1)}, f32[128]{0:T(128)}, u32[]{:S(2)}) copy-start(f32[128]{0:T(128)} %param.29) | copy-start | bytes 1540
  98.0 1.6 %copy-start.6 = (bf16[8192,128]{1,0:T(8,128)(2,1)S(1)}, bf16[8192,128]{1,0:T(8,128)(2,1)}, u32[]{:S(2)}) copy-start(bf16[8192,128]{1,0:T(8,128)(2,1)} %all-gather.4.cloned.1.call-done) | copy-start | bytes 6291460
  99.5 18.6 %copy-start.2 = (bf16[128,2048]{1,0:T(8,128)(2,1)S(1)}, bf16[128,2048]{1,0:T(8,128)(2,1)}, u32[]{:S(2)}) copy-start(bf16[128,2048]{1,0:T(8,128)(2,1)} %wl_ref.1) | copy-start | bytes 1572868
  99.6 18.6 %copy-start.3 = (bf16[128,2048]{1,0:T(8,128)(2,1)S(1)}, bf16[128,2048]{1,0:T(8,128)(2,1)}, u32[]{:S(2)}) copy-start(bf16[128,2048]{1,0:T(8,128)(2,1)} %wa_ref.1) | copy-start | bytes 1572868
  99.6 18.6 %copy-start.5 = (f32[128]{0:T(128)S(1)}, f32[128]{0:T(128)}, u32[]{:S(2)}) copy-start(f32[128]{0:T(128)} %param.35) | copy-start | bytes 1540
  119.9 3.8 %collective-permute-start.1 = (bf16[4,256,256]{2,1,0:T(8,128)(2,1)S(1)}, bf16[4,256,256]{2,1,0:T(8,128)(2,1)S(1)}, u32[]{:S(2)}, u32[]{:S(2)}) collective-permute-start(bf16[4,256,256]{2,1,0:T(8,128)(2,1)S(1)} %get-tuple-element.24), channel_id=1, source_target_pairs={{0,1},{1,0},{2,3},{3,2},{4,5},{5,4},{6,7},{7,6},{8,9},{9,8},{10,11... | collective-permute-start | bytes 1572872 | tf_op jit(solution)/shard_map/ppermute | solution.py:442
Sparse Core Ops, SparseCore 0:
  27.6 70.3 all-gather.3

commit v5 on v4

--- a/solution.py
+++ b/solution.py
@@ -367,8 +367,8 @@
             sum_ref[j] = sum_ref[j] + new
 
     def score_many(i, carry):
-        for k in range(5):
-            score(5 * i + k, False)
+        for k in range(3):
+            score(3 * i + k, False)
         return carry
 
     def score_one(k, carry):
@@ -376,24 +376,24 @@
         return carry
 
     def gather_many(i, carry):
-        gather(*(8 * i + k for k in range(8)))
+        gather(*(4 * i + k for k in range(4)))
         return carry
 
     def gather_one(k, carry):
         gather(k)
         return carry
 
-    many = z // 5
+    many = z // 3
     lax.fori_loop(0, many, score_many, 0)
-    lax.fori_loop(5 * many, z, score_one, 0)
+    lax.fori_loop(3 * many, z, score_one, 0)
     score(z, True)
     for j in range(count):
         best = jnp.max(best_ref[j], axis=1, keepdims=True)
         best = jnp.where(best > 0.5 * NEG, best, 0.0)
         best_ref[j] = jnp.broadcast_to(best, best_ref.shape[1:])
-    many = (z + 1) // 8
+    many = (z + 1) // 4
     lax.fori_loop(0, many, gather_many, 0)
-    lax.fori_loop(8 * many, z + 1, gather_one, 0)
+    lax.fori_loop(4 * many, z + 1, gather_one, 0)
     third = iota((rows, WIDE), 1)
     for j in range(count):
         total = sum_ref[j, :, HEAD_ATT:]
@@ -576,7 +576,7 @@
 def solution(mesh):
     sp, tp = mesh.shape["sp"], mesh.shape["tp"]
     cores = 2
-    ny = math.isqrt(sp) // 2 if sp > 16 else 2
+    ny = math.isqrt(sp) if sp > 16 else 4
     torus = Mesh(mesh.devices.reshape(sp // ny, ny, tp // cores, cores), SP + TP)
     return jax.shard_map(
         body,

time: 147 us -> 151 us (1.027)
  starting transfers between devices: 3.83 us -> 10 us
  blocking collectives: 84.4 us -> 79.5 us
  local copies, waits for them, and re-layouts: 3.54 us -> 5.11 us
    all_to_all x1 -> x0, blocking collectives: 12.8 us -> none  [sent_to_all(): lax.all_to_all(jnp.broadcast_to(a[None], (size, *a.shape)), axis, 0, 0, t...]
    all_to_all x0 -> x1, waiting for transfers between devices: none -> 10.3 us  [sent_to_all(): lax.all_to_all(jnp.broadcast_to(a[None], (size, *a.shape)), axis, 0, 0, t...]
    all_gather x1, waiting for transfers between devices: 11.4 us -> 1.42 us  [body(): keys = lax.all_gather(kv, 'z')]
    all_to_all x1, blocking collectives: 12 us -> 21.5 us  [body(): parts = lax.all_to_all(found, 'y', 0, 0, tiled=True)]
    all_to_all x0 -> x1, starting transfers between devices: none -> 6.06 us  [sent_to_all(): lax.all_to_all(jnp.broadcast_to(a[None], (size, *a.shape)), axis, 0, 0, t...]
  transfers between devices with their start and end apart: 3 -> 4, of which waited for: 3 -> 4; matrix products, arithmetic and copies ran while one was open for 0% -> 0% of each run, Pallas kernels for 9% -> 4%
where the time goes in v5:
time: 151 us; the launch traced here: 149 us
  blocking collectives  79.5 us (53%)
  Pallas kernels  24 us (16%)
  waiting for transfers between devices  15.5 us (10%)
  between operations  13.6 us (9%)
  starting transfers between devices  10 us (7%)
  local copies, waits for them, and re-layouts  5.11 us (3%)
    all_gather x1, blocking collectives, body(): held = lax.all_gather(row_send, 'z')  31.8 us
    pallas_call x7, Pallas kernels, run(): pl.pallas_call(kernel, name=name, out_shape=shapes, in_specs=[smem()] + [...  24 us
    all_to_all x1, blocking collectives, body(): parts = lax.all_to_all(found, 'y', 0, 0, tiled=True)  21.5 us
    all_to_all x1, blocking collectives, body(): own = lax.all_to_all(copies, 'x', 0, 0, tiled=True)  13.7 us
    all_to_all x1, blocking collectives, body(): tiles = lax.all_to_all(pair, 'x', 0, 0, tiled=True)  12.5 us
    all_to_all x1, waiting for transfers between devices, sent_to_all(): lax.all_to_all(jnp.broadcast_to(a[None], (size, *a.shape)), axis, 0, 0, t...  10.3 us
    all_to_all x1, starting transfers between devices, sent_to_all(): lax.all_to_all(jnp.broadcast_to(a[None], (size, *a.shape)), axis, 0, 0, t...  6.06 us
    unnamed x40, local copies, waits for them, and re-layouts  4.11 us
  transfers between devices with their start and end apart: 4, of which 4 were waited for; matrix products, arithmetic and copies ran while one was open for 0% of the time, Pallas kernels for 4%

profile of v5, /device:TPU:480, one launch (start us, length us, event | category | flops | bytes accessed | tf_op | source)
XLA Modules:
  0.0 148.8 jit_solution(12023924108447898044)
XLA Ops:
  6.5 0.1 pad_add_fusion.place_ref
  6.6 0.9 copy-done.12
  7.5 0.0 copy-start.15
  7.5 0.0 copy-start.17
  7.6 0.0 copy-start.18
  7.6 0.6 spread.1
  8.1 0.0 copy-start.7
  8.2 0.0 copy-start.8
  8.2 13.7 %all_to_all.20.own_ref = bf16[4,256,256]{2,1,0:T(8,128)(2,1)S(1)} all-to-all(bf16[4,256,256]{2,1,0:T(8,128)(2,1)S(1)} %spread.1), channel_id=1, replica_groups=mesh['z'=8,'y'=8,'x'=4,'c'=2] {'x'}, dimensions={0} | all-to-all | bytes 1048576 | tf_op jit(solution)/shard_map/all_to_all | solution.py:501
  21.9 2.0 %collective-permute-start = (bf16[4,256,256]{2,1,0:T(8,128)(2,1)S(1)}, bf16[4,256,256]{2,1,0:T(8,128)(2,1)S(1)}, u32[]{:S(2)}, u32[]{:S(2)}) collective-permute-start(bf16[4,256,256]{2,1,0:T(8,128)(2,1)S(1)} %all_to_all.20.own_ref), channel_id=1, source_target_pairs={{0,1},{1,0},{2,3},{3,2},{4,5},{5,4},{6,7},{7,6},{8,9},{9,8},{10,11... | collective-permute-start | bytes 1572872 | tf_op jit(solution)/shard_map/ppermute | solution.py:442
  23.9 1.9 %collective-permute-done.other_ref = bf16[4,256,256]{2,1,0:T(8,128)(2,1)S(1)} collective-permute-done((bf16[4,256,256]{2,1,0:T(8,128)(2,1)S(1)}, bf16[4,256,256]{2,1,0:T(8,128)(2,1)S(1)}, u32[]{:S(2)}, u32[]{:S(2)}) %collective-permute-start) | collective-permute-done | bytes 524320 | tf_op jit(solution)/shard_map/ppermute | solution.py:442
  25.8 0.0 copy-done.9
  25.8 0.0 copy-done.10
  25.8 0.0 copy-done.11
  25.8 0.0 copy-done.13
  25.8 0.0 copy-done.15
  25.8 0.0 copy-done.17
  25.8 0.0 copy-done.18
  25.9 0.0 copy-done.7
  25.9 0.0 copy-done.8
  25.9 0.0 copy-done.4
  25.9 0.6 copy-done.16
  26.5 7.8 %lin.1 = (bf16[400,128]{1,0:T(8,128)(2,1)S(1)}, bf16[16,128]{1,0:T(8,128)(2,1)S(1)}, f32[256,128]{1,0:T(8,128)S(1)}, f32[256,128]{1,0:T(8,128)S(1)}) custom-call(s32[3]{0:T(128)S(1)} %pad_add_fusion.place_ref, bf16[4,256,256]{2,1,0:T(8,128)(2,1)S(1)} %all_to_all.20.own_ref, bf16[4,256,256]{2,1,0:T(8,128)(2,1)S(1)} %collective-permute-done.other_ref, ...), custom_call_target="tpu_custom_call" | custom-call | flops 4000000000 | bytes 4194304 | tf_op jit(solution)/shard_map/lin/pallas_call | solution.py:456
  34.3 1.0 broadcast_in_dim.2
  35.3 6.1 %all-to-all-start.1 = ((bf16[8,400,128]{2,1,0:T(8,128)(2,1)}), bf16[8,400,128]{2,1,0:T(8,128)(2,1)S(1)}, u32[]{:S(2)}, u32[]{:S(2)}) async-start(bf16[8,400,128]{2,1,0:T(8,128)(2,1)} %broadcast_in_dim.2), calls=%async_computation.1 | async-start | bytes 1638400 | tf_op jit(solution)/shard_map/all_to_all | solution.py:438
  41.3 0.0 all-gather.4.cloned.1.call-start
  41.3 0.0 copy-done
  41.4 1.7 %kv.1 = bf16[512,128]{1,0:T(8,128)(2,1)} custom-call(s32[3]{0:T(128)S(1)} %pad_add_fusion.place_ref, bf16[4,256,256]{2,1,0:T(8,128)(2,1)S(1)} %all_to_all.20.own_ref, bf16[4,256,256]{2,1,0:T(8,128)(2,1)S(1)} %collective-permute-done.other_ref, f32[1,2048]{1,0:T(1,128)S(1)} %bitcast.15, bf16[2048,128]{1,0:T(8,128)(2,1)S(1)} %copy-done, ...), custom_call_target="tpu_custom_call" | custom-call | flops 268435456 | bytes 2097152 | tf_op jit(solution)/shard_map/kv/pallas_call | solution.py:456
  43.1 0.0 all-gather.4.cloned.1.call-update
  43.1 10.3 %all-to-all-done.1.gathered_ref.asked_ref = bf16[8,400,128]{2,1,0:T(8,128)(2,1)S(1)} async-done(((bf16[8,400,128]{2,1,0:T(8,128)(2,1)}), bf16[8,400,128]{2,1,0:T(8,128)(2,1)S(1)}, u32[]{:S(2)}, u32[]{:S(2)}) %all-to-all-start.1) | async-done | bytes 819232 | tf_op jit(solution)/shard_map/all_to_all | solution.py:438
  53.4 1.8 %row.1 = (bf16[144,128]{1,0:T(8,128)(2,1)S(1)}, f32[2,128,128]{2,1,0:T(8,128)S(1)}) custom-call(s32[3]{0:T(128)S(1)} %pad_add_fusion.place_ref, bf16[8,400,128]{2,1,0:T(8,128)(2,1)S(1)} %all-to-all-done.1.gathered_ref.asked_ref, bf16[16,128]{1,0:T(8,128)(2,1)S(1)} %get-tuple-element.16.gates_ref), custom_call_target="tpu_custom_call" | custom-call | flops 100000000 | bytes 1048576 | tf_op jit(solution)/shard_map/row/pallas_call | solution.py:456
  55.3 0.0 copy-start.14
  55.3 31.8 %all-gather = bf16[1152,128]{1,0:T(8,128)(2,1)S(1)} all-gather(bf16[144,128]{1,0:T(8,128)(2,1)S(1)} %get-tuple-element.17), channel_id=2, replica_groups=mesh['z'=8,'y'=8,'x'=4,'c'=2] {'z'}, dimensions={0}, use_global_device_ids=true | all-gather | bytes 331776 | tf_op jit(solution)/shard_map/all_gather | solution.py:547
  87.1 0.7 copy-done.19
  87.7 2.3 %mix.1.lin_ref = bf16[256,128]{1,0:T(8,128)(2,1)S(1)} custom-call(s32[3]{0:T(128)S(1)} %pad_add_fusion.place_ref, f32[2,64,64]{2,1,0:T(8,128)S(1)} %copy-done.14, bf16[8,144,128]{2,1,0:T(8,128)(2,1)S(1)} %bitcast.12, f32[2,128,128]{2,1,0:T(8,128)S(1)} %get-tuple-element.18.before_ref, f32[256,128]{1,0:T(8,128)S(1)} %get-tuple-element.19.reach_ref, ...), custom_call_target="tpu_custom_call" | custom-call | flops 1000000000 | bytes 1048576 | tf_op jit(solution)/shard_map/mix/pallas_call | solution.py:456
  90.1 1.4 all-gather.4.cloned.1.call-done
  91.5 1.2 copy-done.6
  92.7 7.7 %att.1 = bf16[8,256,256]{2,1,0:T(8,128)(2,1)S(1)} custom-call(s32[3]{0:T(128)S(1)} %pad_add_fusion.place_ref, bf16[8,400,128]{2,1,0:T(8,128)(2,1)S(1)} %all-to-all-done.1.gathered_ref.asked_ref, bf16[8,144,128]{2,1,0:T(8,128)(2,1)S(1)} %bitcast.13, bf16[8,512,128]{2,1,0:T(8,128)(2,1)S(1)} %bitcast.17), custom_call_target="tpu_custom_call" | custom-call | flops 2147483648 | bytes 4194304 | tf_op jit(solution)/shard_map/att/pallas_call | solution.py:456
  100.5 0.0 copy-start.2
  100.5 0.0 copy-start.3
  100.5 21.5 %all_to_all.21.parts_ref = bf16[8,256,256]{2,1,0:T(8,128)(2,1)S(1)} all-to-all(bf16[8,256,256]{2,1,0:T(8,128)(2,1)S(1)} %att.1), channel_id=1, replica_groups=mesh['z'=8,'y'=8,'x'=4,'c'=2] {'y'}, dimensions={0} | all-to-all | bytes 2097152 | tf_op jit(solution)/shard_map/all_to_all | solution.py:565
  122.0 0.6 copy-done.5
  122.6 2.0 %out.1 = (bf16[4,256,256]{2,1,0:T(8,128)(2,1)S(1)}, bf16[4,256,256]{2,1,0:T(8,128)(2,1)S(1)}) custom-call(s32[3]{0:T(128)S(1)} %pad_add_fusion.place_ref, bf16[8,256,256]{2,1,0:T(8,128)(2,1)S(1)} %all_to_all.21.parts_ref, bf16[256,128]{1,0:T(8,128)(2,1)S(1)} %mix.1.lin_ref, f32[1,128]{1,0:T(1,128)S(1)} %bitcast.16, bf16[128,2048]{1,0:T(8,128)(2,1)S(1)} %copy-done.2, ...), custom_call_target="tpu_custom_call" | custom-call | flops 268435456 | bytes 2097152 | tf_op jit(solution)/shard_map/out/pallas_call | solution.py:456
  124.7 1.9 %collective-permute-start.1 = (bf16[4,256,256]{2,1,0:T(8,128)(2,1)S(1)}, bf16[4,256,256]{2,1,0:T(8,128)(2,1)S(1)}, u32[]{:S(2)}, u32[]{:S(2)}) collective-permute-start(bf16[4,256,256]{2,1,0:T(8,128)(2,1)S(1)} %get-tuple-element.24), channel_id=1, source_target_pairs={{0,1},{1,0},{2,3},{3,2},{4,5},{5,4},{6,7},{7,6},{8,9},{9,8},{10,11... | collective-permute-start | bytes 1572872 | tf_op jit(solution)/shard_map/ppermute | solution.py:442
  126.6 1.9 %collective-permute-done.1 = bf16[4,256,256]{2,1,0:T(8,128)(2,1)S(1)} collective-permute-done((bf16[4,256,256]{2,1,0:T(8,128)(2,1)S(1)}, bf16[4,256,256]{2,1,0:T(8,128)(2,1)S(1)}, u32[]{:S(2)}, u32[]{:S(2)}) %collective-permute-start.1) | collective-permute-done | bytes 524320 | tf_op jit(solution)/shard_map/ppermute | solution.py:442
  128.5 0.1 add_convert_fusion
  128.6 12.5 %all_to_all.22 = bf16[4,256,256]{2,1,0:T(8,128)(2,1)S(1)} all-to-all(bf16[4,256,256]{2,1,0:T(8,128)(2,1)S(1)} %add_convert_fusion), channel_id=1, replica_groups=mesh['z'=8,'y'=8,'x'=4,'c'=2] {'x'}, dimensions={0} | all-to-all | bytes 1048576 | tf_op jit(solution)/shard_map/all_to_all | solution.py:572
  141.2 0.7 reduce_sum.12
  (16 shorter events, 0.0 us)
Async XLA Ops:
  6.6 0.9 copy-start.12
  7.5 18.3 %copy-start.9 = (bf16[2048,128]{1,0:T(8,128)(2,1)S(1)}, bf16[2048,128]{1,0:T(8,128)(2,1)}, u32[]{:S(2)}) copy-start(bf16[2048,128]{1,0:T(8,128)(2,1)} %wv_ref.2) | copy-start | bytes 1572868
  7.5 18.3 %copy-start.10 = (bf16[2048,128]{1,0:T(8,128)(2,1)S(1)}, bf16[2048,128]{1,0:T(8,128)(2,1)}, u32[]{:S(2)}) copy-start(bf16[2048,128]{1,0:T(8,128)(2,1)} %wq_ref.1) | copy-start | bytes 1572868
  7.5 18.3 %copy-start.11 = (bf16[2048,64]{0,1:T(8,128)(2,1)S(1)}, bf16[2048,64]{0,1:T(8,128)(2,1)}, u32[]{:S(2)}) copy-start(bf16[2048,64]{0,1:T(8,128)(2,1)} %param.24) | copy-start | bytes 786436
  7.5 18.3 %copy-start.13 = (f32[256,128]{1,0:T(8,128)S(1)}, f32[256,128]{1,0:T(8,128)}, u32[]{:S(2)}) copy-start(f32[256,128]{1,0:T(8,128)} %shift_ref.1) | copy-start | bytes 393220
  7.5 18.3 %copy-start.15 = (bf16[64,128]{1,0:T(8,128)(2,1)S(1)}, bf16[64,128]{1,0:T(8,128)(2,1)}, u32[]{:S(2)}) copy-start(bf16[64,128]{1,0:T(8,128)(2,1)} %up_ref.1) | copy-start | bytes 49156
  7.5 18.3 %copy-start.17 = (f32[128]{0:T(128)S(1)}, f32[128]{0:T(128)}, u32[]{:S(2)}) copy-start(f32[128]{0:T(128)} %param.26) | copy-start | bytes 1540
  7.6 18.3 %copy-start.18 = (f32[128]{0:T(128)S(1)}, f32[128]{0:T(128)}, u32[]{:S(2)}) copy-start(f32[128]{0:T(128)} %param.28) | copy-start | bytes 1540
  8.1 17.7 %copy-start.7 = (bf16[2048,128]{1,0:T(8,128)(2,1)S(1)}, bf16[2048,128]{1,0:T(8,128)(2,1)}, u32[]{:S(2)}) copy-start(bf16[2048,128]{1,0:T(8,128)(2,1)} %wr_ref.1) | copy-start | bytes 1572868
  8.2 17.7 %copy-start.8 = (bf16[2048,128]{1,0:T(8,128)(2,1)S(1)}, bf16[2048,128]{1,0:T(8,128)(2,1)}, u32[]{:S(2)}) copy-start(bf16[2048,128]{1,0:T(8,128)(2,1)} %wk_ref.2) | copy-start | bytes 1572868
  21.9 4.0 %copy-start.4 = (f32[2048]{0:T(1024)S(1)}, f32[2048]{0:T(1024)}, u32[]{:S(2)}) copy-start(f32[2048]{0:T(1024)} %param.20) | copy-start | bytes 24580
  21.9 3.9 %collective-permute-start = (bf16[4,256,256]{2,1,0:T(8,128)(2,1)S(1)}, bf16[4,256,256]{2,1,0:T(8,128)(2,1)S(1)}, u32[]{:S(2)}, u32[]{:S(2)}) collective-permute-start(bf16[4,256,256]{2,1,0:T(8,128)(2,1)S(1)} %all_to_all.20.own_ref), channel_id=1, source_target_pairs={{0,1},{1,0},{2,3},{3,2},{4,5},{5,4},{6,7},{7,6},{8,9},{9,8},{10,11... | collective-permute-start | bytes 1572872 | tf_op jit(solution)/shard_map/ppermute | solution.py:442
  25.8 0.7 copy-start.16
  35.3 6.1 %copy-start = (bf16[2048,128]{1,0:T(8,128)(2,1)S(1)}, bf16[2048,128]{1,0:T(8,128)(2,1)}, u32[]{:S(2)}) copy-start(bf16[2048,128]{1,0:T(8,128)(2,1)} %wk_ref.3) | copy-start | bytes 1572868
  35.3 6.1 %copy-start.1 = (bf16[2048,128]{1,0:T(8,128)(2,1)S(1)}, bf16[2048,128]{1,0:T(8,128)(2,1)}, u32[]{:S(2)}) copy-start(bf16[2048,128]{1,0:T(8,128)(2,1)} %wv_ref.3) | copy-start | bytes 1572868
  35.3 18.1 %all-to-all-start.1 = ((bf16[8,400,128]{2,1,0:T(8,128)(2,1)}), bf16[8,400,128]{2,1,0:T(8,128)(2,1)S(1)}, u32[]{:S(2)}, u32[]{:S(2)}) async-start(bf16[8,400,128]{2,1,0:T(8,128)(2,1)} %broadcast_in_dim.2), calls=%async_computation.1 | async-start | bytes 1638400 | tf_op jit(solution)/shard_map/all_to_all | solution.py:438
  41.3 50.2 %all-gather.4.cloned.1.call-start = ((), (), s32[]{:S(2)}) async-start(), calls=%async_computation.4 | async-start | bytes 1179648 | tf_op jit(solution)/shard_map/all_gather | solution.py:506
  55.3 31.8 %copy-start.14 = (f32[2,64,64]{2,1,0:T(8,128)S(1)}, f32[2,64,64]{2,1,0:T(8,128)}, u32[]{:S(2)}) copy-start(f32[2,64,64]{2,1,0:T(8,128)} %state_ref.1) | copy-start | bytes 98308
  87.1 0.7 copy-start.19
  91.5 1.2 copy-start.6
  100.5 21.5 %copy-start.2 = (bf16[128,2048]{1,0:T(8,128)(2,1)S(1)}, bf16[128,2048]{1,0:T(8,128)(2,1)}, u32[]{:S(2)}) copy-start(bf16[128,2048]{1,0:T(8,128)(2,1)} %wl_ref.1) | copy-start | bytes 1572868
  100.5 21.5 %copy-start.3 = (bf16[128,2048]{1,0:T(8,128)(2,1)S(1)}, bf16[128,2048]{1,0:T(8,128)(2,1)}, u32[]{:S(2)}) copy-start(bf16[128,2048]{1,0:T(8,128)(2,1)} %wa_ref.1) | copy-start | bytes 1572868
  122.0 0.7 copy-start.5
  124.7 3.8 %collective-permute-start.1 = (bf16[4,256,256]{2,1,0:T(8,128)(2,1)S(1)}, bf16[4,256,256]{2,1,0:T(8,128)(2,1)S(1)}, u32[]{:S(2)}, u32[]{:S(2)}) collective-permute-start(bf16[4,256,256]{2,1,0:T(8,128)(2,1)S(1)} %get-tuple-element.24), channel_id=1, source_target_pairs={{0,1},{1,0},{2,3},{3,2},{4,5},{5,4},{6,7},{7,6},{8,9},{9,8},{10,11... | collective-permute-start | bytes 1572872 | tf_op jit(solution)/shard_map/ppermute | solution.py:442
Sparse Core Ops, SparseCore 0:
  44.2 47.2 all-gather.3
